TPU v7x, 128 devices: a whole 4x4x4 slice. The times are simulated.
128 devices in a mesh: rep: 2 (over z_hi), fs: 32 (over z_lo, y, x), tp: 2 (over core).
Axes of the slice: x: 4, y: 4, z: 4 (z_hi: 2, z_lo: 2; z = z_hi * 2 + z_lo), core: 2. Of those that a mesh axis runs over, the one named last changes fastest.
Arguments:
- tokens: bfloat16 [49152, 2048], P(('rep', 'fs', 'tp')), may hold values from -6 to 6
- outer_weight: float32 [2048, 1536], P('fs', 'tp'), may hold values from -0.125 to 0.125
- inner_weight: float32 [2048, 1536], P('fs', 'tp'), may hold values from -0.125 to 0.125
- value_weight: float32 [2048, 1536], P('fs', 'tp'), may hold values from -0.125 to 0.125
- conv_taps: float32 [3, 1536], P(None, 'tp'), may hold values from -3 to 3
- mix_out: float32 [1536, 2048], P('tp', 'fs'), may hold values from -0.15625 to 0.15625
- norm_first: float32 [2048], replicated, may hold values from 0.1 to 1.9
- up_weight: float32 [2048, 4096], P('fs', 'tp'), may hold values from -0.125 to 0.125
- down_weight: float32 [4096, 2048], P('tp', 'fs'), may hold values from -0.09375 to 0.09375
- norm_second: float32 [2048], replicated, may hold values from 0.1 to 1.9
Outputs:
- encoded: bfloat16 [49152, 2048], P(('rep', 'fs', 'tp'))
All inputs are finite; a program needn't handle non-finite values.
Results may differ from a plain program's by a relative error of at most 0.015.
Values may be sent and summed in bfloat16 or wider, within the bound.
A program may use at most 128 MiB of HBM per device.

v0:
```python
import jax
import jax.numpy as jnp
from jax import lax
from jax.sharding import Mesh
from jax.sharding import PartitionSpec as P

SEQ = 128
FS = ("fs_0", "fs_1", "fs_2")
REP_FS_TP = ("rep", "fs_0", "fs_1", "fs_2", "tp")


residual_scale = 2.0**0.25
norm_epsilon = 1e-05


def in_one_piece(arrays, axis, dim, along):
    ends, at = ([], 0)
    for a in arrays[:-1]:
        at += a.shape[along]
        ends.append(at)
    both = jnp.concatenate(arrays, axis=along)
    return tuple(jnp.split(lax.all_gather(both, axis, axis=dim, tiled=True), ends, axis=along))


def laid_out(tiles, dim):
    tiles = jnp.moveaxis(tiles, 0, dim)
    lengths = tiles.shape
    return tiles.reshape(*lengths[:dim], lengths[dim] * lengths[dim + 1], *lengths[dim + 2 :])


def stacked_from(x, axes, order):
    tiles = x
    for k in order:
        tiles = lax.all_gather(tiles, axes[k])
    done = order[::-1]
    back = [done.index(k) for k in range(len(axes))]
    tiles = tiles.transpose(*back, *range(len(axes), tiles.ndim))
    return tiles.reshape(-1, *x.shape)


def whole_of(x, axes, order, dim):
    return laid_out(stacked_from(x, axes, order), dim)


def cut_along(x, dim, length):
    before, after = (x.shape[:dim], x.shape[dim + 1 :])
    return jnp.moveaxis(x.reshape(*before, length, -1, *after), dim, 0)


def sum_at_owner(x, axis, dim):
    tiles = cut_along(x, dim, lax.axis_size(axis))
    arrived = lax.all_to_all(tiles, axis, split_axis=0, concat_axis=0, tiled=True)
    return arrived.astype(jnp.float32).sum(axis=0)


def layer_norm(values, scaling):
    center = values - jnp.mean(values, axis=-1, keepdims=True)
    spread = jnp.mean(center * center, axis=-1, keepdims=True)
    return center * lax.rsqrt(spread + norm_epsilon) * scaling


def short_conv(product, conv_taps):
    places = jnp.arange(product.shape[0], dtype=jnp.int32) % SEQ
    blank = jnp.zeros((1, product.shape[1]), jnp.float32)
    before = jnp.concatenate([blank, product[:-1]], axis=0)
    after = jnp.concatenate([product[1:], blank], axis=0)
    before = jnp.where((places > 0)[:, None], before, 0.0)
    after = jnp.where((places < SEQ - 1)[:, None], after, 0.0)
    return conv_taps[0] * before + conv_taps[1] * product + conv_taps[2] * after


def local(
    tokens,
    outer_weight,
    inner_weight,
    value_weight,
    conv_taps,
    mix_out,
    norm_first,
    up_weight,
    down_weight,
    norm_second,
):
    grouped = lax.all_gather(tokens, "tp", axis=0, tiled=True)
    outer_bf = outer_weight.astype(jnp.bfloat16)
    inner_bf = inner_weight.astype(jnp.bfloat16)
    value_bf = value_weight.astype(jnp.bfloat16)
    outer_full, inner_full, value_full = in_one_piece((outer_bf, inner_bf, value_bf), FS, 0, 1)
    outer = jnp.dot(grouped, outer_full, preferred_element_type=jnp.float32)
    inner = jnp.dot(grouped, inner_full, preferred_element_type=jnp.float32)
    value = jnp.dot(grouped, value_full, preferred_element_type=jnp.float32)
    mixed = (outer * short_conv(inner * value, conv_taps)).astype(jnp.bfloat16)
    mixout_full = whole_of(mix_out.astype(jnp.bfloat16), FS, (0, 1, 2), 1)
    selected = mixed
    mixing = sum_at_owner(
        jnp.dot(selected, mixout_full, preferred_element_type=jnp.float32).astype(jnp.bfloat16),
        "tp",
        0,
    )
    first = layer_norm(residual_scale * tokens.astype(jnp.float32) + mixing, norm_first).astype(
        jnp.bfloat16
    )
    grouped_first = lax.all_gather(first, "tp", axis=0, tiled=True)
    upward_bf = up_weight.astype(jnp.bfloat16)
    upward_full = lax.all_gather(upward_bf, FS, axis=0, tiled=True)
    raised = jnp.dot(grouped_first, upward_full, preferred_element_type=jnp.float32)
    raised = jax.nn.relu(raised)
    hidden = (raised * raised).astype(jnp.bfloat16)
    down_full = lax.all_gather(down_weight.astype(jnp.bfloat16), FS, axis=1, tiled=True)
    selected = hidden
    lowered = sum_at_owner(
        jnp.dot(selected, down_full, preferred_element_type=jnp.float32).astype(jnp.bfloat16),
        "tp",
        0,
    )
    return layer_norm(residual_scale * first.astype(jnp.float32) + lowered, norm_second).astype(
        jnp.bfloat16
    )


def solution(mesh):
    finer = Mesh(
        mesh.devices.reshape(mesh.shape["rep"], 2, 4, 4, mesh.shape["tp"]),
        ("rep", "fs_0", "fs_1", "fs_2", "tp"),
    )
    placed = (
        P(REP_FS_TP, None),
        P(FS, "tp"),
        P(FS, "tp"),
        P(FS, "tp"),
        P(None, "tp"),
        P("tp", FS),
        P(),
        P(FS, "tp"),
        P("tp", FS),
        P(),
    )
    return jax.shard_map(
        local, mesh=finer, in_specs=placed, out_specs=P(REP_FS_TP, None), check_vma=False
    )
```

profile of v0, /device:TPU:0, one launch (start us, length us, event | category | flops | bytes accessed | tf_op | source)
XLA Modules:
  0.0 636.6 jit_solution(7984287710747323062)
XLA Ops:
  6.5 0.0 copy-start.4
  6.5 0.0 copy-start.5
  6.5 0.0 copy-start.6
  6.5 0.0 copy-start.2
  6.5 0.0 all-gather.20.cloned.1.call-start
  6.6 1.0 convert_element_type.53
  7.6 5.5 all-gather
  13.1 0.0 copy-start.9
  13.1 14.6 %all-gather.1 = bf16[8,768,64]{1,2,0:T(8,128)(2,1)} all-gather(bf16[2,768,64]{1,2,0:T(8,128)(2,1)S(1)} %bitcast.37), channel_id=3, replica_groups=mesh['rep'=2,'fs_0'=2,'fs_1'=4,'fs_2'=4,'tp'=2] {'fs_1'}, dimensions={0}, use_global_device_ids=true | all-gather | bytes 983040 | tf_op jit(solution)/shard_map/all_gather | solution.py:34
  27.7 0.0 all-gather.20.cloned.1.call-update
  27.7 0.0 all-gather.12.cloned.1.call-start
  27.8 0.7 all-gather.12.cloned.1.call-update
  28.5 0.0 all-gather.10.cloned.1.call-start
  28.5 0.0 copy-done.4
  28.6 0.0 copy-done.5
  28.6 0.0 copy-done.6
  28.6 0.7 pad_maximum_fusion
  29.4 0.0 all-gather.10.cloned.1.call-update
  29.4 0.0 all-gather.16.cloned.1.call-start
  29.4 0.0 copy-done.2
  29.4 0.7 convert_element_type.58
  30.2 0.0 all-gather.16.cloned.1.call-update
  30.2 0.0 all-gather.14.cloned.1.call-start
  30.3 0.0 copy-done.9
  30.3 39.4 %all-gather.20.cloned.1.call-done = bf16[16,2,768,64]{2,3,1,0:T(8,128)(2,1)} async-done(((bf16[4,2,768,64]{2,3,1,0:T(8,128)(2,1)}), bf16[16,2,768,64]{2,3,1,0:T(8,128)(2,1)}) %all-gather.20.cloned.1.call-update) | async-done | bytes 3145744 | tf_op jit(solution)/shard_map/all_gather | solution.py:34
  69.7 3.9 copy.15
  73.6 12.8 %all-gather.12.cloned.1.call-done = bf16[768,2048]{1,0:T(8,128)(2,1)} async-done(((bf16[384,2048]{1,0:T(8,128)(2,1)}), bf16[768,2048]{1,0:T(8,128)(2,1)}) %all-gather.12.cloned.1.call-update) | async-done | bytes 3145744 | tf_op jit(solution)/shard_map/all_gather | solution.py:84
  86.4 170.8 %all-gather.10.cloned.1.call-done = bf16[2048,2304]{1,0:T(8,128)(2,1)} async-done(((bf16[64,2304]{1,0:T(8,128)(2,1)}), bf16[2048,2304]{1,0:T(8,128)(2,1)}) %all-gather.10.cloned.1.call-update) | async-done | bytes 9437200 | tf_op jit(solution)/shard_map/all_gather | solution.py:22
  257.2 0.0 copy-start.10
  257.2 5.7 fusion
  262.8 0.0 copy-done.10
  262.8 4.6 multiply_bitcast_fusion
  267.4 2.9 fusion.21
  270.3 13.9 %convolution_convert_fusion.1 = bf16[768,2048]{1,0:T(8,128)(2,1)} fusion(bf16[768,2048]{0,1:T(8,128)(2,1)} %bitcast.32, f32[767,768]{0,1:T(8,128)} %get-tuple-element.9, f32[768,768]{0,1:T(8,128)S(1)} %multiply_bitcast_fusion, f32[767,768]{0,1:T(8,128)} %get-tuple-element.8, bf16[768,2048]{1,0:T(8,128)(2,1)} %all-gather.12.cloned.1.call-done, ...), kind=kOutput, calls=%fused_computation.4 | convolution fusion | flops 4838719488 | bytes 19671552 | tf_op jit(solution)/shard_map/dot_general | solution.py:96
  284.3 7.6 %all_to_all.10 = bf16[2,384,2048]{2,1,0:T(8,128)(2,1)S(1)} all-to-all(bf16[2,384,2048]{2,1,0:T(8,128)(2,1)} %bitcast.33), channel_id=1, replica_groups=mesh['rep'=2,'fs_0'=2,'fs_1'=4,'fs_2'=4,'tp'=2] {'tp'}, dimensions={0} | all-to-all | bytes 6291456 | tf_op jit(solution)/shard_map/all_to_all | solution.py:52
  291.8 0.0 copy-start.1
  291.8 0.7 convert_reduce_fusion.1
  292.6 0.7 copy-done.1
  293.2 0.5 fusion.11
  293.7 0.0 copy-start.7
  293.7 0.7 multiply_reduce_fusion.1
  294.5 0.0 copy-done.7
  294.5 0.0 copy-start.3
  294.5 1.8 multiply_convert_fusion.2
  296.3 0.0 all-gather.14.cloned.1.call-update
  296.3 0.0 all-gather.18.cloned.1.call-start
  296.4 0.0 copy-done.3
  296.4 0.8 convert_element_type.60
  297.2 0.0 all-gather.18.cloned.1.call-update
  297.2 126.8 %all-gather.16.cloned.1.call-done = bf16[2048,2048]{1,0:T(8,128)(2,1)} async-done(((bf16[64,2048]{1,0:T(8,128)(2,1)}), bf16[2048,2048]{1,0:T(8,128)(2,1)}) %all-gather.16.cloned.1.call-update) | async-done | bytes 8388624 | tf_op jit(solution)/shard_map/all_gather | solution.py:105
  424.0 16.9 %all-gather.14.cloned.1.call-done = bf16[768,2048]{1,0:T(8,128)(2,1)} async-done(((bf16[384,2048]{1,0:T(8,128)(2,1)}), bf16[768,2048]{1,0:T(8,128)(2,1)}) %all-gather.14.cloned.1.call-update) | async-done | bytes 3145744 | tf_op jit(solution)/shard_map/all_gather | solution.py:103
  440.9 10.0 %multiply_convert_fusion = bf16[768,2048]{1,0:T(8,128)(2,1)S(1)} fusion(bf16[768,2048]{1,0:T(8,128)(2,1)} %all-gather.14.cloned.1.call-done, bf16[2048,2048]{1,0:T(8,128)(2,1)} %all-gather.16.cloned.1.call-done), kind=kOutput, calls=%fused_computation.1 | convolution fusion | flops 6447169536 | bytes 14680064 | tf_op jit(solution)/shard_map/dot_general | solution.py:106
  450.9 159.0 %all-gather.18.cloned.1.call-done = bf16[2048,2048]{0,1:T(8,128)(2,1)} async-done(((bf16[2048,64]{0,1:T(8,128)(2,1)}), bf16[2048,2048]{0,1:T(8,128)(2,1)}) %all-gather.18.cloned.1.call-update) | async-done | bytes 8388624 | tf_op jit(solution)/shard_map/all_gather | solution.py:109
  609.9 9.1 %convolution_convert_fusion = bf16[768,2048]{1,0:T(8,128)(2,1)S(1)} fusion(bf16[768,2048]{1,0:T(8,128)(2,1)S(1)} %multiply_convert_fusion, bf16[2048,2048]{0,1:T(8,128)(2,1)} %all-gather.18.cloned.1.call-done), kind=kOutput, calls=%fused_computation.3 | convolution fusion | flops 6444023808 | bytes 14680064 | tf_op jit(solution)/shard_map/dot_general | solution.py:112
  619.1 6.3 all_to_all.11
  625.3 0.0 copy-start
  625.3 0.7 convert_reduce_fusion
  626.1 0.7 copy-done
  626.7 0.5 fusion.12
  627.2 0.0 copy-start.8
  627.2 0.7 multiply_reduce_fusion
  627.9 0.0 copy-done.8
  627.9 1.8 multiply_convert_fusion.1
  (10 shorter events, 0.1 us)
Async XLA Ops:
  6.5 22.0 %copy-start.4 = (f32[64,768]{1,0:T(8,128)S(1)}, f32[64,768]{1,0:T(8,128)}, u32[]{:S(2)}) copy-start(f32[64,768]{1,0:T(8,128)} %param.11) | copy-start | bytes 589828
  6.5 22.0 %copy-start.5 = (f32[64,768]{1,0:T(8,128)S(1)}, f32[64,768]{1,0:T(8,128)}, u32[]{:S(2)}) copy-start(f32[64,768]{1,0:T(8,128)} %param.12) | copy-start | bytes 589828
  6.5 22.1 %copy-start.6 = (f32[64,768]{1,0:T(8,128)S(1)}, f32[64,768]{1,0:T(8,128)}, u32[]{:S(2)}) copy-start(f32[64,768]{1,0:T(8,128)} %param.13) | copy-start | bytes 589828
  6.5 22.9 %copy-start.2 = (f32[64,2048]{1,0:T(8,128)S(1)}, f32[64,2048]{1,0:T(8,128)}, u32[]{:S(2)}) copy-start(f32[64,2048]{1,0:T(8,128)} %param.17) | copy-start | bytes 1572868
  6.5 63.1 %all-gather.20.cloned.1.call-start = ((), (), s32[]{:S(2)}) async-start(), calls=%async_computation.7 | async-start | bytes 3932160 | tf_op jit(solution)/shard_map/all_gather | solution.py:34
  13.1 17.1 %copy-start.9 = (f32[3,768]{1,0:T(4,128)S(1)}, f32[3,768]{1,0:T(4,128)}, u32[]{:S(2)}) copy-start(f32[3,768]{1,0:T(4,128)} %param.14) | copy-start | bytes 27652
  27.7 58.6 %all-gather.12.cloned.1.call-start = ((), (), s32[]{:S(2)}) async-start(), calls=%async_computation.3 | async-start | bytes 4718592 | tf_op jit(solution)/shard_map/all_gather | solution.py:84
  28.5 228.7 %all-gather.10.cloned.1.call-start = ((), (), s32[]{:S(2)}) async-start(), calls=%async_computation.2 | async-start | bytes 9732096 | tf_op jit(solution)/shard_map/all_gather | solution.py:22
  29.4 394.6 %all-gather.16.cloned.1.call-start = ((), (), s32[]{:S(2)}) async-start(), calls=%async_computation.5 | async-start | bytes 8650752 | tf_op jit(solution)/shard_map/all_gather | solution.py:105
  30.2 410.7 %all-gather.14.cloned.1.call-start = ((), (), s32[]{:S(2)}) async-start(), calls=%async_computation.4 | async-start | bytes 4718592 | tf_op jit(solution)/shard_map/all_gather | solution.py:103
  257.2 5.7 copy-start.10
  291.8 1.4 copy-start.1
  293.7 0.7 copy-start.7
  294.5 1.9 copy-start.3
  296.3 313.6 %all-gather.18.cloned.1.call-start = ((), (), s32[]{:S(2)}) async-start(), calls=%async_computation.6 | async-start | bytes 8650752 | tf_op jit(solution)/shard_map/all_gather | solution.py:109
  625.3 1.4 copy-start
  627.2 0.7 copy-start.8
Sparse Core Ops, SparseCore 0:
  27.8 41.7 all-gather.19
  71.3 14.9 all-gather.11
  88.0 169.1 all-gather.9
  258.7 165.2 all-gather.15
  425.5 15.3 all-gather.13
  442.4 167.5 all-gather.17
where the time goes:
time: 638 us; the launch traced here: 637 us
  waiting for transfers between devices  526 us (82%)
  matrix products  43.3 us (7%)
  blocking collectives  33.9 us (5%)
  between operations  13.7 us (2%)
  other arithmetic  10.8 us (2%)
  local copies, waits for them, and re-layouts  8.27 us (1%)
    all_gather x1, waiting for transfers between devices, in_one_piece(): lax.all_gather(both, axis, axis=dim, tiled=True)  171 us
    all_gather x1, waiting for transfers between devices, local(): lax.all_gather(down_weight.astype(jnp.bfloat16), FS, axis=1, tiled=True)  159 us
    all_gather x1, waiting for transfers between devices, local(): upward_full = lax.all_gather(upward_bf, FS, axis=0, tiled=True)  127 us
    all_gather x1, waiting for transfers between devices, stacked_from(): tiles = lax.all_gather(tiles, axes[k])  39.4 us
    all_gather x2, blocking collectives, stacked_from(): tiles = lax.all_gather(tiles, axes[k])  20.1 us
    all_gather x1, waiting for transfers between devices, local(): grouped_first = lax.all_gather(first, 'tp', axis=0, tiled=True)  16.9 us
    dot_general x1, matrix products, local(): jnp.dot(selected, mixout_full, preferred_element_type=jnp.float32)  13.9 us
    all_to_all x2, blocking collectives, sum_at_owner(): lax.all_to_all(tiles, axis, split_axis=0, concat_axis=0, tiled=True)  13.8 us
  transfers between devices with their start and end apart: 6, of which 6 were waited for; matrix products, arithmetic and copies ran while one was open for 7% of the time, Pallas kernels for 0%

commit v1 on v0

v1 whole, which is shorter than its diff:
```python
import jax
import jax.numpy as jnp
from jax import lax
from jax.experimental import pallas as pl
from jax.experimental.pallas import tpu as pltpu
from jax.sharding import Mesh
from jax.sharding import PartitionSpec as P

SEQ = 128
FS = ("fs_0", "fs_1", "fs_2")
REP_FS_TP = ("rep", "fs_0", "fs_1", "fs_2", "tp")
MESH = pl.DeviceIdType.MESH
SCALE = 2.0**0.25
EPS = 1e-05
F32 = jnp.float32
BF16 = jnp.bfloat16

D = 2048
ROWS = 64
TOK = 384
CH = 384
HID = 1024
NSEQ = TOK // SEQ
WIDTHS = (3 * CH, CH, HID, HID)
PROJ, MIX, UP, DOWN = range(4)


def kernel(
    tok, pin, min_, uin, din, taps, gain1, gain2, out,
    wp, wm, wu, wd, x, f, mixed, hid, pd, d_send, d_recv, z_send, z_recv, acc,
    sw_send, sw_recv, sw_own, sz_send, sz_recv, sx_own, sx_send, sx_recv, sf_send, sf_recv,
    sd_send, sd_recv, sr_send, sr_recv, s_out,
):
    rep, zl = lax.axis_index("rep"), lax.axis_index("fs_0")
    my_y, my_x, core = lax.axis_index("fs_1"), lax.axis_index("fs_2"), lax.axis_index("tp")
    z = rep * 2 + zl

    def device(z_, y_, x_, c_):
        return (z_ // 2, z_ % 2, y_, x_, c_)

    z_plus, z_minus = (z + 1) % 4, (z + 3) % 4
    above, below = device(z_plus, my_y, my_x, core), device(z_minus, my_y, my_x, core)
    sibling = device(z, my_y, my_x, 1 - core)
    z_to = (z + 3 + 2 * core) % 4
    z_from = (z + 1 + 2 * core) % 4
    helper, helped = device(z_to, my_y, my_x, core), device(z_from, my_y, my_x, core)
    x_plus, x_minus = device(z, my_y, (my_x + 1) % 4, core), device(z, my_y, (my_x + 3) % 4, core)
    y_plus, y_minus = device(z, (my_y + 1) % 4, my_x, core), device(z, (my_y + 3) % 4, my_x, core)

    weights = (wp, wm, wu, wd)
    shards = (pin, min_, uin, din)
    own_row = pl.multiple_of(((zl * 4 + my_y) * 4 + my_x) * ROWS, ROWS)

    def block_row(color, i1, i2):
        y_, x_ = (i2, i1) if color == 0 else (i1, i2)
        return pl.multiple_of(((color * 4 + y_) * 4 + x_) * ROWS, ROWS)

    me = ((my_x, my_y), (my_y, my_x))
    plus = ((x_plus, y_plus), (y_plus, x_plus))
    minus = ((x_minus, y_minus), (y_minus, x_minus))
    SHIFT = (0, 3, 1, 2)

    def block(color, k1, k2):
        return block_row(color, (me[color][0] + SHIFT[k1]) % 4, (me[color][1] + SHIFT[k2]) % 4)

    def wcopy(t, color, slot, row, rows, target):
        part = weights[t].at[pl.ds(row, rows)]
        return pltpu.make_async_remote_copy(
            src_ref=part, dst_ref=part, send_sem=sw_send.at[t], recv_sem=sw_recv.at[t, color, slot],
            device_id=target, device_id_type=MESH,
        )

    HALF = ROWS // 2

    def first_leg(t, color):
        row = block(color, 0, 0)
        wcopy(t, color, 0, row, ROWS, plus[color][0]).start()
        wcopy(t, color, 1, row, ROWS, minus[color][0]).start()

    def second_leg(t, color, k):
        row = block(color, k, 0)
        wcopy(t, color, 4 + 4 * k, row, ROWS, plus[color][1]).start()
        wcopy(t, color, 5 + 4 * k, row, ROWS, minus[color][1]).start()

    def arrive(t, color, slot, row, rows):
        wcopy(t, color, slot, row, rows, plus[color][0]).wait_recv()

    def zcopy(t, half, row, target):
        return pltpu.make_async_remote_copy(
            src_ref=shards[t].at[1 - zl, pl.ds(half * HALF, HALF)],
            dst_ref=weights[t].at[pl.ds(row + half * HALF, HALF)],
            send_sem=sz_send.at[t, half], recv_sem=sz_recv.at[t, half],
            device_id=target, device_id_type=MESH,
        )

    other_row = pl.multiple_of((((1 - zl) * 4 + my_y) * 4 + my_x) * ROWS, ROWS)

    def own_copy(t):
        return pltpu.make_async_copy(shards[t].at[zl], weights[t].at[pl.ds(own_row, ROWS)], sw_own.at[t])

    def start_z(t):
        zcopy(t, 0, own_row, above).start()
        zcopy(t, 1, own_row, below).start()

    def g0(t):
        own_copy(t).wait()
        zcopy(t, 0, other_row, above).wait_recv()
        zcopy(t, 1, other_row, below).wait_recv()
        for color in (0, 1):
            first_leg(t, color)
        for color in (0, 1):
            second_leg(t, color, 0)

    def g1(t):
        for color in (0, 1):
            row = block(color, 1, 0)
            arrive(t, color, 0, row, ROWS)
            wcopy(t, color, 2, row, HALF, plus[color][0]).start()
        for color in (0, 1):
            row = block(color, 2, 0)
            arrive(t, color, 1, row, ROWS)
            wcopy(t, color, 3, row + HALF, HALF, minus[color][0]).start()
        for color in (0, 1):
            second_leg(t, color, 1)
            second_leg(t, color, 2)

    def g2(t):
        for color in (0, 1):
            row = block(color, 3, 0)
            arrive(t, color, 2, row, HALF)
            arrive(t, color, 3, row + HALF, HALF)
            second_leg(t, color, 3)

    def g3(t, k):
        for color in (0, 1):
            row = block(color, k, 1)
            arrive(t, color, 4 + 4 * k, row, ROWS)
            wcopy(t, color, 6 + 4 * k, row, HALF, plus[color][1]).start()
            row = block(color, k, 2)
            arrive(t, color, 5 + 4 * k, row, ROWS)
            wcopy(t, color, 7 + 4 * k, row + HALF, HALF, minus[color][1]).start()

    def g4(t):
        for k in range(4):
            for color in (0, 1):
                row = block(color, k, 3)
                arrive(t, color, 6 + 4 * k, row, HALF)
                arrive(t, color, 7 + 4 * k, row + HALF, HALF)

    def seq(s):
        return pl.ds(s * SEQ, SEQ)

    def tok_z(s):
        return pltpu.make_async_remote_copy(
            src_ref=tok.at[seq(s)], dst_ref=x.at[2, seq(s)], send_sem=sx_send.at[0],
            recv_sem=sx_recv.at[1 + s], device_id=helper, device_id_type=MESH,
        )

    def tok_sibling():
        return pltpu.make_async_remote_copy(
            src_ref=tok, dst_ref=x.at[1], send_sem=sx_send.at[1],
            recv_sem=sx_recv.at[0], device_id=sibling, device_id_type=MESH,
        )

    def tok_relay(s):
        return pltpu.make_async_remote_copy(
            src_ref=x.at[2, seq(s)], dst_ref=x.at[3, seq(s)], send_sem=sx_send.at[2],
            recv_sem=sx_recv.at[4 + s], device_id=sibling, device_id_type=MESH,
        )

    def first_copy(kind, s):
        source, target, to = ((0, 1, sibling), (0, 2, helper), (2, 3, sibling))[kind]
        return pltpu.make_async_remote_copy(
            src_ref=f.at[source, seq(s)], dst_ref=f.at[target, seq(s)], send_sem=sf_send.at[kind],
            recv_sem=sf_recv.at[kind, s], device_id=to, device_id_type=MESH,
        )

    def part_copy(phase, slot, s):
        return pltpu.make_async_remote_copy(
            src_ref=d_send.at[slot, seq(s)], dst_ref=d_recv.at[slot, seq(s)], send_sem=sd_send.at[phase, slot],
            recv_sem=sd_recv.at[phase, slot, s], device_id=sibling, device_id_type=MESH,
        )

    def sum_copy(phase, s):
        return pltpu.make_async_remote_copy(
            src_ref=z_send.at[seq(s)], dst_ref=z_recv.at[seq(s)], send_sem=sr_send.at[phase],
            recv_sem=sr_recv.at[phase, s], device_id=helped, device_id_type=MESH,
        )

    def relay_tokens(s):
        tok_z(s).wait_recv()
        tok_relay(s).start()

    def all_sent(ref, sem):
        pltpu.make_async_remote_copy(
            src_ref=ref, dst_ref=ref, send_sem=sem, recv_sem=sw_recv.at[0, 0, 0], device_id=x_plus, device_id_type=MESH
        ).wait_send()

    row_id = lax.broadcasted_iota(jnp.int32, (SEQ, 1), 0)

    def convolve(g, at, ch, c0):
        for s in range(NSEQ):
            rows = pl.ds(s * SEQ, SEQ)
            product = pd[rows, pl.ds(ch, ch)] * pd[rows, pl.ds(2 * ch, ch)]
            before = jnp.where(row_id > 0, pltpu.roll(product, 1, 0), 0.0)
            after = jnp.where(row_id < SEQ - 1, pltpu.roll(product, SEQ - 1, 0), 0.0)
            conv = taps[0:1, c0:c0 + ch] * before + taps[1:2, c0:c0 + ch] * product + taps[2:3, c0:c0 + ch] * after
            mixed[g, rows, c0:c0 + ch] = (pd[rows, pl.ds(0, ch)] * conv).astype(BF16)

    def project(g):
        pd[...] = jnp.dot(x[g], wp[:, 0:768], preferred_element_type=F32)
        convolve(g, 0, 256, 0)
        pd[:, 0:384] = jnp.dot(x[g], wp[:, 768:1152], preferred_element_type=F32)
        convolve(g, 768, 128, 256)

    def times_transposed(rows_of, w, emit):
        def step(j, _):
            cols = pl.ds(pl.multiple_of(j * 512, 512), 512)
            emit(cols, lax.dot_general(rows_of(), w[cols, :], (((1,), (1,)), ((), ())), preferred_element_type=F32))
            return 0

        lax.fori_loop(0, D // 512, step, 0)

    def partial_sums(phase, source, w, g, s=None):
        rows = pl.ds(0, TOK) if s is None else seq(s)
        parts = range(NSEQ) if s is None else (s,)
        slot = g // 2
        if g in (1, 3):

            def emit(cols, total):
                d_send[slot, rows, cols] = total.astype(BF16)

        else:
            for part in parts:
                part_copy(phase, slot, part).wait_recv()

            def emit(cols, total):
                total = total + d_recv[slot, rows, cols].astype(F32)
                if g == 2:
                    z_send[rows, cols] = total.astype(BF16)
                else:
                    acc[rows, cols] = total

        times_transposed(lambda: source[g, rows, :], w, emit)
        for part in parts:
            if g in (1, 3):
                part_copy(phase, slot, part).start()
            elif g == 2:
                sum_copy(phase, part).start()

    def normed(phase, base, gain, s, target):
        sum_copy(phase, s).wait_recv()
        step_rows = 32

        def step(i, _):
            rows = pl.ds(pl.multiple_of(s * SEQ + i * step_rows, step_rows), step_rows)
            v = SCALE * base[0, rows, :].astype(F32) + (acc[rows, :] + z_recv[rows, :].astype(F32))
            center = v - jnp.mean(v, axis=-1, keepdims=True)
            spread = jnp.mean(center * center, axis=-1, keepdims=True)
            target(rows, (center * lax.rsqrt(spread + EPS) * gain[...]).astype(BF16))
            return 0

        lax.fori_loop(0, SEQ // step_rows, step, 0)

    def to_first(rows, value):
        f[0, rows, :] = value

    def to_result(rows, value):
        z_send[rows, :] = value

    def expand(g):
        def step(j, _):
            cols = pl.ds(pl.multiple_of(j * 512, 512), 512)
            raised = jnp.maximum(jnp.dot(f[g], wu[:, cols], preferred_element_type=F32), 0.0)
            hid[g, :, cols] = (raised * raised).astype(BF16)
            return 0

        lax.fori_loop(0, HID // 512, step, 0)

    barrier = pltpu.get_barrier_semaphore()
    for other in (x_plus, x_minus, y_plus, y_minus, above, below, sibling):
        pl.semaphore_signal(barrier, inc=1, device_id=other, device_id_type=MESH)
    own_tokens = pltpu.make_async_copy(tok, x.at[0], sx_own)
    for t in range(4):
        own_copy(t).start()
    own_tokens.start()
    pl.semaphore_wait(barrier, 7)

    start_z(PROJ)
    start_z(MIX)
    tok_z(0).start()
    start_z(UP)
    tok_z(1).start()
    start_z(DOWN)
    tok_z(2).start()
    tok_sibling().start()

    g0(PROJ)
    g1(PROJ)
    g3(PROJ, 0)
    relay_tokens(0)
    g2(PROJ)
    g3(PROJ, 1)
    relay_tokens(1)
    g3(PROJ, 2)
    g0(MIX)
    relay_tokens(2)
    g3(PROJ, 3)
    g0(UP)
    g1(MIX)
    g3(MIX, 0)
    g4(PROJ)
    for s in range(NSEQ):
        tok_relay(s).wait_recv()
    project(3)
    g2(MIX)
    g3(MIX, 1)
    g3(MIX, 2)
    g1(UP)
    g3(MIX, 3)
    g3(UP, 0)
    project(2)
    g4(MIX)
    for s in range(NSEQ):
        partial_sums(0, mixed, wm, 3, s)
    for s in range(NSEQ):
        partial_sums(0, mixed, wm, 2, s)
    g2(UP)
    g3(UP, 1)
    tok_sibling().wait_recv()
    project(1)
    g3(UP, 2)
    g0(DOWN)
    g3(UP, 3)
    partial_sums(0, mixed, wm, 1)
    own_tokens.wait()
    project(0)
    g1(DOWN)
    g3(DOWN, 0)
    partial_sums(0, mixed, wm, 0)
    g4(UP)
    for s in range(NSEQ):
        normed(0, x, gain1, s, to_first)
        first_copy(1, s).start()
        first_copy(0, s).start()
        if s == 0:
            g2(DOWN)
            g3(DOWN, 1)
        if s == 1:
            g3(DOWN, 2)
            g3(DOWN, 3)
    expand(0)
    for s in range(NSEQ):
        first_copy(0, s).wait_recv()
    expand(1)
    for s in range(NSEQ):
        first_copy(1, s).wait_recv()
        first_copy(2, s).start()
    expand(2)
    for s in range(NSEQ):
        first_copy(2, s).wait_recv()
    expand(3)
    for slot in (0, 1):
        all_sent(d_send.at[slot], sd_send.at[0, slot])
    all_sent(z_send, sr_send.at[0])
    g4(DOWN)
    for s in range(NSEQ):
        partial_sums(1, hid, wd, 3, s)
    for s in range(NSEQ):
        partial_sums(1, hid, wd, 2, s)
    partial_sums(1, hid, wd, 1)
    partial_sums(1, hid, wd, 0)
    all_sent(z_send, sr_send.at[1])
    results = []
    for s in range(NSEQ):
        normed(1, f, gain2, s, to_result)
        results.append(pltpu.make_async_copy(z_send.at[seq(s)], out.at[seq(s)], s_out.at[s]))
        results[-1].start()

    for t in range(4):
        all_sent(weights[t].at[pl.ds(0, 30 * ROWS)], sw_send.at[t])
        zcopy(t, 0, own_row, above).wait_send()
        zcopy(t, 1, own_row, below).wait_send()
    for kind in range(3):
        all_sent(x.at[0], sx_send.at[kind])
        all_sent(f.at[0], sf_send.at[kind])
    for slot in (0, 1):
        all_sent(d_send.at[slot], sd_send.at[1, slot])
    for result in results:
        result.wait()


def local(tokens, outer_weight, inner_weight, value_weight, conv_taps, mix_out, norm_first, up_weight, down_weight, norm_second):
    o, i, v = (w.astype(BF16) for w in (outer_weight, inner_weight, value_weight))
    halves = []
    for h in (0, 1):
        a, b, c = h * CH, h * CH + 256, (h + 1) * CH
        halves.append(jnp.concatenate([w[:, a:b] for w in (o, i, v)] + [w[:, b:c] for w in (o, i, v)], axis=1))
    pin = jnp.stack(halves)

    def split(w, width):
        return w.astype(BF16).reshape(ROWS, 2, width).transpose(1, 0, 2)

    min_ = split(mix_out.T, CH)
    uin = split(up_weight, HID)
    din = split(down_weight.T, HID)
    zl = lax.axis_index("fs_0")
    taps = lax.dynamic_slice_in_dim(conv_taps, zl * CH, CH, axis=1)

    hbm = pl.BlockSpec(memory_space=pl.ANY)
    vmem = pl.BlockSpec(memory_space=pltpu.VMEM)
    dma = pltpu.SemaphoreType.DMA
    return pl.pallas_call(
        kernel,
        name="mixer_ffn",
        out_shape=jax.ShapeDtypeStruct((TOK, D), BF16),
        in_specs=[hbm] * 5 + [vmem] * 3,
        out_specs=hbm,
        scratch_shapes=[pltpu.VMEM((D, w), BF16) for w in WIDTHS]
        + [
            pltpu.VMEM((4, TOK, D), BF16),
            pltpu.VMEM((4, TOK, D), BF16),
            pltpu.VMEM((4, TOK, CH), BF16),
            pltpu.VMEM((4, TOK, HID), BF16),
            pltpu.VMEM((TOK, 768), F32),
            pltpu.VMEM((2, TOK, D), BF16),
            pltpu.VMEM((2, TOK, D), BF16),
            pltpu.VMEM((TOK, D), BF16),
            pltpu.VMEM((TOK, D), BF16),
            pltpu.VMEM((TOK, D), F32),
            dma((4,)),
            dma((4, 2, 20)),
            dma((4,)),
            dma((4, 2)),
            dma((4, 2)),
            dma,
            dma((3,)),
            dma((7,)),
            dma((3,)),
            dma((3, 3)),
            dma((2, 2)),
            dma((2, 2, 3)),
            dma((2,)),
            dma((2, 3)),
            dma((3,)),
        ],
        compiler_params=pltpu.CompilerParams(
            collective_id=0, has_side_effects=True, vmem_limit_bytes=62 * 1024 * 1024
        ),
    )(tokens, pin, min_, uin, din, taps, norm_first.reshape(1, D), norm_second.reshape(1, D))


def solution(mesh):
    finer = Mesh(
        mesh.devices.reshape(mesh.shape["rep"], 2, 4, 4, mesh.shape["tp"]),
        ("rep", "fs_0", "fs_1", "fs_2", "tp"),
    )
    placed = (
        P(REP_FS_TP, None),
        P(FS, "tp"),
        P(FS, "tp"),
        P(FS, "tp"),
        P(None, "tp"),
        P("tp", FS),
        P(),
        P(FS, "tp"),
        P("tp", FS),
        P(),
    )
    return jax.shard_map(
        local, mesh=finer, in_specs=placed, out_specs=P(REP_FS_TP, None), check_vma=False
    )
```

time: 638 us -> 147 us (0.23)
  waiting for transfers between devices: 526 us -> 0 us
  Pallas kernels: 0 us -> 136 us
  matrix products: 43.3 us -> 0 us
  blocking collectives: 33.9 us -> 0 us
  between operations: 13.7 us -> 0.07 us
    all_gather x6 -> x0, waiting for transfers between devices: 526 us -> none  [the longest x1 171 us: in_one_piece(): lax.all_gather(both, axis, axis=dim, tiled=True)]
    pallas_call x0 -> x1, Pallas kernels: none -> 136 us  [local(): pl.pallas_call(kernel, name='mixer_ffn', out_shape=jax.ShapeDtypeStruct((...]
    dot_general x5 -> x0, matrix products: 43.3 us -> none  [the longest x1 13.9 us: local(): jnp.dot(selected, mixout_full, preferred_element_type=jnp.float32)]
    all_gather x2 -> x0, blocking collectives: 20.1 us -> none  [stacked_from(): tiles = lax.all_gather(tiles, axes[k])]
    all_to_all x2 -> x0, blocking collectives: 13.8 us -> none  [sum_at_owner(): lax.all_to_all(tiles, axis, split_axis=0, concat_axis=0, tiled=True)]
  transfers between devices with their start and end apart: 6 -> 0, of which waited for: 6 -> 0; matrix products, arithmetic and copies ran while one was open for 7% -> 0% of each run, Pallas kernels for 0% -> 0%
where the time goes in v1:
time: 147 us
  Pallas kernels  136 us (93%)
  local copies, waits for them, and re-layouts  5.57 us (4%)
  other arithmetic  4.57 us (3%)
    pallas_call x1, Pallas kernels, local(): pl.pallas_call(kernel, name='mixer_ffn', out_shape=jax.ShapeDtypeStruct((...  136 us
    unnamed x12, local copies, waits for them, and re-layouts  3.49 us

profile of v1, /device:TPU:0, one launch (start us, length us, event | category | flops | bytes accessed | tf_op | source)
XLA Modules:
  0.0 146.5 jit_solution(10426768548478039636)
XLA Ops:
  0.0 0.0 copy-start
  0.0 0.0 copy-start.2
  0.0 0.0 copy-start.1
  0.0 0.7 copy-done
  0.7 0.6 constant_dynamic-slice_fusion.taps
  1.3 0.9 convert_element_type.24
  2.2 0.9 convert_element_type.25
  3.2 0.9 convert_element_type.26
  4.1 0.9 convert_element_type.27
  5.1 0.6 copy.20
  5.7 0.0 copy-done.1
  5.8 0.0 copy-done.2
  5.8 0.8 bitcast_bitcast_fusion
  6.7 0.7 pad_maximum_fusion.pin
  7.5 136.3 %mixer_ffn.1 = bf16[384,2048]{1,0:T(8,128)(2,1)} custom-call(bf16[384,2048]{1,0:T(8,128)(2,1)} %tok.1, bf16[2,64,1152]{2,1,0:T(8,128)(2,1)} %pad_maximum_fusion.pin, bf16[2,64,384]{2,1,0:T(8,128)(2,1)} %bitcast.26, bf16[2,64,1024]{2,1,0:T(8,128)(2,1)} %get-tuple-element.18.uin, bf16[2,64,1024]{2,1,0:T(8,128)(2,1)} %get-tuple-element.17.din, ...), custom_call_target="tpu_custom_call" | custom-call | tf_op jit(solution)/shard_map/mixer_ffn/pallas_call | solution.py:413
  143.8 2.7 %copy.32 = bf16[384,2048]{1,0:T(8,128)(2,1)} copy(bf16[384,2048]{1,0:T(8,128)(2,1)} %mixer_ffn.1) | data formatting | bytes 3145728
  (8 shorter events, 0.1 us)
Async XLA Ops:
  0.0 0.7 copy-start
  0.0 5.8 %copy-start.2 = (f32[2048,64]{0,1:T(8,128)S(1)}, f32[2048,64]{0,1:T(8,128)}, u32[]{:S(2)}) copy-start(f32[2048,64]{0,1:T(8,128)} %param.18) | copy-start | bytes 1572868
  0.0 5.7 %copy-start.1 = (f32[64,2048]{1,0:T(8,128)S(1)}, f32[64,2048]{1,0:T(8,128)}, u32[]{:S(2)}) copy-start(f32[64,2048]{1,0:T(8,128)} %param.17) | copy-start | bytes 1572868

commit v2 on v1

v2 whole, which is shorter than its diff:
```python
import jax
import jax.numpy as jnp
from jax import lax
from jax.experimental import pallas as pl
from jax.experimental.pallas import tpu as pltpu
from jax.sharding import Mesh
from jax.sharding import PartitionSpec as P

SEQ = 128
FS = ("fs_0", "fs_1", "fs_2")
REP_FS_TP = ("rep", "fs_0", "fs_1", "fs_2", "tp")
MESH = pl.DeviceIdType.MESH
SCALE = 2.0**0.25
EPS = 1e-05
F32 = jnp.float32
BF16 = jnp.bfloat16

D = 2048
ROWS = 64
TOK = 384
CH = 384
HID = 1024
NSEQ = TOK // SEQ
WIDTHS = (CH, 3 * CH, HID, HID)
MIX, PROJ, UP, DOWN = range(4)
COLS = 512
NCOL = D // COLS


def kernel(
    tok, wo_in, wi_in, wv_in, wm_in, wu_in, wd_in, taps, gain1, gain2, out,
    wm, wp, wu, wd, wm2, gm, gp, gu, gd, stage_p, stage_m, stage_u, stage_d,
    x, f, mixed, mixed2, hid, pd, d_send, d_recv, z_send, z_recv, acc,
    s_in, sw_send, sw_recv, sz_send, sz_recv, sx_own, sx_send, sx_recv, sf_send, sf_recv,
    sq_send, sq_recv, sm_send, sm_recv, sd_send, sd_recv, sr_send, sr_recv, s_out,
):
    rep, zl = lax.axis_index("rep"), lax.axis_index("fs_0")
    my_y, my_x, core = lax.axis_index("fs_1"), lax.axis_index("fs_2"), lax.axis_index("tp")
    z = rep * 2 + zl

    def device(z_, y_, x_, c_):
        return (z_ // 2, z_ % 2, y_, x_, c_)

    z_plus, z_minus = (z + 1) % 4, (z + 3) % 4
    above, below = device(z_plus, my_y, my_x, core), device(z_minus, my_y, my_x, core)
    sibling = device(z, my_y, my_x, 1 - core)
    z_to = (z + 3 + 2 * core) % 4
    z_from = (z + 1 + 2 * core) % 4
    helper, helped = device(z_to, my_y, my_x, core), device(z_from, my_y, my_x, core)
    x_plus, x_minus = device(z, my_y, (my_x + 1) % 4, core), device(z, my_y, (my_x + 3) % 4, core)
    y_plus, y_minus = device(z, (my_y + 1) % 4, my_x, core), device(z, (my_y + 3) % 4, my_x, core)

    def remote(src, dst, send_sem, recv_sem, target):
        return pltpu.make_async_remote_copy(
            src_ref=src, dst_ref=dst, send_sem=send_sem, recv_sem=recv_sem, device_id=target, device_id_type=MESH
        )

    weights = (wm, wp, wu, wd)
    given = (gm, gp, gu, gd)
    own_row = pl.multiple_of(((zl * 4 + my_y) * 4 + my_x) * ROWS, ROWS)
    other_row = pl.multiple_of((((1 - zl) * 4 + my_y) * 4 + my_x) * ROWS, ROWS)

    def load(which):
        pairs = (
            (wm_in, stage_m), (wo_in, stage_p.at[0]), (wi_in, stage_p.at[1]), (wv_in, stage_p.at[2]),
            (wu_in, stage_u), (wd_in, stage_d),
        )
        return pltpu.make_async_copy(*pairs[which], s_in.at[which])

    def cast(t):
        keep, give = weights[t], given[t]
        rows = pl.ds(own_row, ROWS)
        if t == PROJ:
            for which in (1, 2, 3):
                load(which).wait()
            for width, c0, at in ((256, 0, 0), (128, 256, 768)):
                for i in range(3):
                    mine = pl.ds(pl.multiple_of(zl * CH + c0, 128), width)
                    theirs = pl.ds(pl.multiple_of((1 - zl) * CH + c0, 128), width)
                    cols = slice(at + i * width, at + (i + 1) * width)
                    keep[rows, cols] = stage_p[i, :, mine].astype(BF16)
                    give[:, cols] = stage_p[i, :, theirs].astype(BF16)
        else:
            stage = {MIX: stage_m, UP: stage_u, DOWN: stage_d}[t]
            load({MIX: 0, UP: 4, DOWN: 5}[t]).wait()
            width = WIDTHS[t]
            keep[rows, :] = stage[:, pl.ds(pl.multiple_of(zl * width, 128), width)].astype(BF16)
            give[...] = stage[:, pl.ds(pl.multiple_of((1 - zl) * width, 128), width)].astype(BF16)

    me = ((my_x, my_y), (my_y, my_x))
    plus = ((x_plus, y_plus), (y_plus, x_plus))
    minus = ((x_minus, y_minus), (y_minus, x_minus))
    SHIFT = (0, 3, 1, 2)
    HALF = ROWS // 2

    def block(color, k1, k2):
        i1, i2 = (me[color][0] + SHIFT[k1]) % 4, (me[color][1] + SHIFT[k2]) % 4
        y_, x_ = (i2, i1) if color == 0 else (i1, i2)
        return pl.multiple_of(((color * 4 + y_) * 4 + x_) * ROWS, ROWS)

    def wcopy(t, color, slot, row, rows, target):
        part = weights[t].at[pl.ds(row, rows)]
        return remote(part, part, sw_send.at[t], sw_recv.at[t, color, slot], target)

    def second_leg(t, color, k):
        row = block(color, k, 0)
        wcopy(t, color, 4 + 4 * k, row, ROWS, plus[color][1]).start()
        wcopy(t, color, 5 + 4 * k, row, ROWS, minus[color][1]).start()

    def arrive(t, color, slot, row, rows):
        wcopy(t, color, slot, row, rows, plus[color][0]).wait_recv()

    def zcopy(t, half, row, target):
        return remote(
            given[t].at[pl.ds(half * HALF, HALF)], weights[t].at[pl.ds(row + half * HALF, HALF)],
            sz_send.at[t, half], sz_recv.at[t, half], target,
        )

    def start_z(t):
        zcopy(t, 0, own_row, above).start()
        zcopy(t, 1, own_row, below).start()

    def both_legs(t, color, row):
        for slot, step in ((0, 1), (1, 3)):
            wcopy(t, color, slot, row, ROWS, device(z, (my_y + step * color) % 4, (my_x + step * (1 - color)) % 4, core)).start()
        for slot, step in ((4, 1), (5, 3)):
            wcopy(t, color, slot, row, ROWS, device(z, (my_y + step * (1 - color)) % 4, (my_x + step * color) % 4, core)).start()

    def g0_own(t):
        both_legs(t, zl, own_row)

    def g0_other(t):
        zcopy(t, 0, other_row, above).wait_recv()
        zcopy(t, 1, other_row, below).wait_recv()
        both_legs(t, 1 - zl, other_row)

    def g1(t):
        for color in (0, 1):
            row = block(color, 1, 0)
            arrive(t, color, 0, row, ROWS)
            wcopy(t, color, 2, row, HALF, plus[color][0]).start()
        for color in (0, 1):
            row = block(color, 2, 0)
            arrive(t, color, 1, row, ROWS)
            wcopy(t, color, 3, row + HALF, HALF, minus[color][0]).start()
        for color in (0, 1):
            second_leg(t, color, 1)
            second_leg(t, color, 2)

    def g2(t):
        for color in (0, 1):
            row = block(color, 3, 0)
            arrive(t, color, 2, row, HALF)
            arrive(t, color, 3, row + HALF, HALF)
            second_leg(t, color, 3)

    def g3(t, k):
        for color in (0, 1):
            row = block(color, k, 1)
            arrive(t, color, 4 + 4 * k, row, ROWS)
            wcopy(t, color, 6 + 4 * k, row, HALF, plus[color][1]).start()
            row = block(color, k, 2)
            arrive(t, color, 5 + 4 * k, row, ROWS)
            wcopy(t, color, 7 + 4 * k, row + HALF, HALF, minus[color][1]).start()

    def g4(t):
        for k in range(4):
            for color in (0, 1):
                row = block(color, k, 3)
                arrive(t, color, 6 + 4 * k, row, HALF)
                arrive(t, color, 7 + 4 * k, row + HALF, HALF)

    def mix_swap(color):
        rows = pl.ds(color * 1024, 1024)
        return remote(wm.at[rows], wm2.at[rows], sq_send.at[color], sq_recv.at[color], (above, below)[color])

    def seq(s):
        return pl.ds(s * SEQ, SEQ)

    def tok_z(s):
        return remote(tok.at[seq(s)], x.at[2, seq(s)], sx_send.at[0], sx_recv.at[1 + s], helper)

    def tok_sibling():
        return remote(tok, x.at[1], sx_send.at[1], sx_recv.at[0], sibling)

    def tok_relay(s):
        return remote(x.at[2, seq(s)], x.at[3, seq(s)], sx_send.at[2], sx_recv.at[4 + s], sibling)

    def first_copy(kind, s):
        source, target, to = ((0, 1, sibling), (0, 2, helper), (2, 3, sibling))[kind]
        return remote(f.at[source, seq(s)], f.at[target, seq(s)], sf_send.at[kind], sf_recv.at[kind, s], to)

    def mixed_copy(i):
        return remote(mixed.at[2 + i], mixed2.at[i], sm_send.at[i], sm_recv.at[i], (helped, helper)[i])

    def part_copy(phase, slot, j):
        return remote(d_send.at[slot, j], d_recv.at[slot, j], sd_send.at[phase, slot], sd_recv.at[phase, slot, j], sibling)

    def sum_copy(j):
        return remote(z_send.at[j], z_recv.at[j], sr_send, sr_recv.at[j], helped)

    def relay_tokens(s):
        tok_z(s).wait_recv()
        tok_relay(s).start()

    def all_sent(ref, sem):
        remote(ref, ref, sem, sw_recv.at[0, 0, 0], x_plus).wait_send()

    row_id = lax.broadcasted_iota(jnp.int32, (SEQ, 1), 0)

    def convolve(g, ch, c0):
        tap = [taps[k:k + 1, pl.ds(pl.multiple_of(zl * CH + c0, 128), ch)] for k in range(3)]
        for s in range(NSEQ):
            rows = pl.ds(s * SEQ, SEQ)
            product = pd[rows, pl.ds(ch, ch)] * pd[rows, pl.ds(2 * ch, ch)]
            before = jnp.where(row_id > 0, pltpu.roll(product, 1, 0), 0.0)
            after = jnp.where(row_id < SEQ - 1, pltpu.roll(product, SEQ - 1, 0), 0.0)
            conv = tap[0] * before + tap[1] * product + tap[2] * after
            mixed[g, rows, c0:c0 + ch] = (pd[rows, pl.ds(0, ch)] * conv).astype(BF16)

    def project(g):
        pd[...] = jnp.dot(x[g], wp[:, 0:768], preferred_element_type=F32)
        convolve(g, 256, 0)
        pd[:, 0:384] = jnp.dot(x[g], wp[:, 768:1152], preferred_element_type=F32)
        convolve(g, 128, 256)

    def dot_t(rows, w, j):
        return lax.dot_general(
            rows, w[j * COLS:(j + 1) * COLS, :], (((1,), (1,)), ((), ())), preferred_element_type=F32
        )

    def mix_sums(g):
        for j in range(NCOL):
            total = dot_t(mixed[g], wm, j) + dot_t(mixed2[g], wm2, j)
            if g == 1:
                d_send[0, j] = total.astype(BF16)
                part_copy(0, 0, j).start()
            else:
                acc[:, j * COLS:(j + 1) * COLS] = total

    def ffn_sums(g, j):
        total = dot_t(hid[g], wd, j)
        slot = g // 2
        if g in (1, 3):
            d_send[slot, j] = total.astype(BF16)
            part_copy(1, slot, j).start()
        else:
            part_copy(1, slot, j).wait_recv()
            total = total + d_recv[slot, j].astype(F32)
            if g == 2:
                z_send[j] = total.astype(BF16)
                sum_copy(j).start()
            else:
                acc[:, j * COLS:(j + 1) * COLS] = total

    def normed(base, arrived, gain, s, target):
        step_rows = 32

        def step(i, _):
            rows = pl.ds(pl.multiple_of(s * SEQ + i * step_rows, step_rows), step_rows)
            came = jnp.concatenate([arrived(j, rows) for j in range(NCOL)], axis=1)
            v = SCALE * base[0, rows, :].astype(F32) + (acc[rows, :] + came)
            center = v - jnp.mean(v, axis=-1, keepdims=True)
            spread = jnp.mean(center * center, axis=-1, keepdims=True)
            target[0, rows, :] = (center * lax.rsqrt(spread + EPS) * gain[...]).astype(BF16)
            return 0

        lax.fori_loop(0, SEQ // step_rows, step, 0)

    def expand(g, s=None):
        rows = pl.ds(0, TOK) if s is None else seq(s)

        def step(j, _):
            cols = pl.ds(pl.multiple_of(j * 512, 512), 512)
            raised = jnp.maximum(jnp.dot(f[g, rows, :], wu[:, cols], preferred_element_type=F32), 0.0)
            hid[g, rows, cols] = (raised * raised).astype(BF16)
            return 0

        lax.fori_loop(0, HID // 512, step, 0)

    barrier = pltpu.get_barrier_semaphore()
    for other in (x_plus, x_minus, y_plus, y_minus, above, below, sibling):
        pl.semaphore_signal(barrier, inc=1, device_id=other, device_id_type=MESH)
    own_tokens = pltpu.make_async_copy(tok, x.at[0], sx_own)
    for which in range(6):
        load(which).start()
    own_tokens.start()
    for t in range(4):
        cast(t)
    pl.semaphore_wait(barrier, 7)

    start_z(MIX)
    start_z(PROJ)
    g0_own(MIX)
    g0_own(PROJ)
    tok_z(0).start()
    tok_sibling().start()
    start_z(UP)
    tok_z(1).start()
    tok_z(2).start()
    start_z(DOWN)
    g0_other(MIX)
    g0_other(PROJ)
    g1(MIX)
    g3(MIX, 0)
    g2(MIX)
    g1(PROJ)
    g3(MIX, 1)
    g3(MIX, 2)
    g3(MIX, 3)
    g3(PROJ, 0)
    relay_tokens(0)
    g4(MIX)
    mix_swap(0).start()
    mix_swap(1).start()
    g2(PROJ)
    g3(PROJ, 1)
    relay_tokens(1)
    g3(PROJ, 2)
    relay_tokens(2)
    g3(PROJ, 3)
    g0_own(UP)
    g0_other(UP)
    for s in range(NSEQ):
        tok_relay(s).wait_recv()
    g4(PROJ)
    project(3)
    mixed_copy(1).start()
    g1(UP)
    g3(UP, 0)
    project(2)
    mixed_copy(0).start()
    tok_sibling().wait_recv()
    g2(UP)
    g3(UP, 1)
    project(1)
    g3(UP, 2)
    mix_swap(0).wait_recv()
    mix_swap(1).wait_recv()
    mixed_copy(1).wait_recv()
    mix_sums(1)
    g3(UP, 3)
    g0_own(DOWN)
    g0_other(DOWN)
    own_tokens.wait()
    project(0)
    mixed_copy(0).wait_recv()
    mix_sums(0)
    for j in range(NCOL):
        part_copy(0, 0, j).wait_recv()
    for s in range(NSEQ):
        normed(x, lambda j, rows: d_recv[0, j, rows, :].astype(F32), gain1, s, f)
        first_copy(1, s).start()
        first_copy(0, s).start()
    g4(UP)
    g1(DOWN)
    g3(DOWN, 0)
    expand(0)
    g2(DOWN)
    g3(DOWN, 1)
    for s in range(NSEQ):
        first_copy(0, s).wait_recv()
    expand(1)
    g3(DOWN, 2)
    all_sent(d_send.at[0], sd_send.at[0, 0])
    for s in range(NSEQ):
        first_copy(1, s).wait_recv()
        first_copy(2, s).start()
        expand(2, s)
        if s == 0:
            g3(DOWN, 3)
        first_copy(2, s).wait_recv()
        expand(3, s)
    g4(DOWN)
    ffn_sums(3, 0)
    ffn_sums(3, 1)
    ffn_sums(2, 0)
    ffn_sums(3, 2)
    ffn_sums(2, 1)
    ffn_sums(3, 3)
    ffn_sums(2, 2)
    ffn_sums(2, 3)
    for j in range(NCOL):
        ffn_sums(1, j)
    for j in range(NCOL):
        ffn_sums(0, j)
    for j in range(NCOL):
        sum_copy(j).wait_recv()
    results = []
    for s in range(NSEQ):
        normed(f, lambda j, rows: z_recv[j, rows, :].astype(F32), gain2, s, x)
        results.append(pltpu.make_async_copy(x.at[0, seq(s)], out.at[seq(s)], s_out.at[s]))
        results[-1].start()

    for t in range(4):
        all_sent(weights[t].at[pl.ds(0, 30 * ROWS)], sw_send.at[t])
        zcopy(t, 0, own_row, above).wait_send()
        zcopy(t, 1, own_row, below).wait_send()
    for kind in range(3):
        all_sent(x.at[0], sx_send.at[kind])
        all_sent(f.at[0], sf_send.at[kind])
    for i in (0, 1):
        mix_swap(i).wait_send()
        mixed_copy(i).wait_send()
        all_sent(d_send.at[i], sd_send.at[1, i])
    all_sent(z_send, sr_send)
    for result in results:
        result.wait()


def local(tokens, outer_weight, inner_weight, value_weight, conv_taps, mix_out, norm_first, up_weight, down_weight, norm_second):
    hbm = pl.BlockSpec(memory_space=pl.ANY)
    vmem = pl.BlockSpec(memory_space=pltpu.VMEM)
    dma = pltpu.SemaphoreType.DMA
    return pl.pallas_call(
        kernel,
        name="mixer_ffn",
        out_shape=jax.ShapeDtypeStruct((TOK, D), BF16),
        in_specs=[hbm] * 7 + [vmem] * 3,
        out_specs=hbm,
        scratch_shapes=[pltpu.VMEM((D, w), BF16) for w in WIDTHS]
        + [pltpu.VMEM((D, CH), BF16)]
        + [pltpu.VMEM((ROWS, w), BF16) for w in WIDTHS]
        + [
            pltpu.VMEM((3, ROWS, 2 * CH), F32),
            pltpu.VMEM((ROWS, 2 * CH), F32),
            pltpu.VMEM((ROWS, 2 * HID), F32),
            pltpu.VMEM((ROWS, 2 * HID), F32),
            pltpu.VMEM((4, TOK, D), BF16),
            pltpu.VMEM((4, TOK, D), BF16),
            pltpu.VMEM((4, TOK, CH), BF16),
            pltpu.VMEM((2, TOK, CH), BF16),
            pltpu.VMEM((4, TOK, HID), BF16),
            pltpu.VMEM((TOK, 768), F32),
            pltpu.VMEM((2, NCOL, TOK, COLS), BF16),
            pltpu.VMEM((2, NCOL, TOK, COLS), BF16),
            pltpu.VMEM((NCOL, TOK, COLS), BF16),
            pltpu.VMEM((NCOL, TOK, COLS), BF16),
            pltpu.VMEM((TOK, D), F32),
            dma((6,)),
            dma((4,)),
            dma((4, 2, 20)),
            dma((4, 2)),
            dma((4, 2)),
            dma,
            dma((3,)),
            dma((7,)),
            dma((3,)),
            dma((3, 3)),
            dma((2,)),
            dma((2,)),
            dma((2,)),
            dma((2,)),
            dma((2, 2)),
            dma((2, 2, 4)),
            dma,
            dma((4,)),
            dma((3,)),
        ],
        compiler_params=pltpu.CompilerParams(
            collective_id=0, has_side_effects=True, vmem_limit_bytes=62 * 1024 * 1024
        ),
    )(
        tokens, outer_weight, inner_weight, value_weight, mix_out.T, up_weight, down_weight.T,
        conv_taps, norm_first.reshape(1, D), norm_second.reshape(1, D),
    )


def solution(mesh):
    finer = Mesh(
        mesh.devices.reshape(mesh.shape["rep"], 2, 4, 4, mesh.shape["tp"]),
        ("rep", "fs_0", "fs_1", "fs_2", "tp"),
    )
    placed = (
        P(REP_FS_TP, None),
        P(FS, "tp"),
        P(FS, "tp"),
        P(FS, "tp"),
        P(None, "tp"),
        P("tp", FS),
        P(),
        P(FS, "tp"),
        P("tp", FS),
        P(),
    )
    return jax.shard_map(
        local, mesh=finer, in_specs=placed, out_specs=P(REP_FS_TP, None), check_vma=False
    )
```

time: 147 us -> 120 us (0.82)
  Pallas kernels: 136 us -> 118 us
  other arithmetic: 4.57 us -> 0 us
  local copies, waits for them, and re-layouts: 5.57 us -> 2.73 us
    pallas_call x1, Pallas kernels: 136 us -> 118 us  [local(): pl.pallas_call(kernel, name='mixer_ffn', out_shape=jax.ShapeDtypeStruct((...]
    convert_element_type x6 -> x0, other arithmetic: 3.82 us -> none  [the longest x3 2.82 us: local(): w.astype(BF16)]
    unnamed x12 -> x1, local copies, waits for them, and re-layouts: 3.49 us -> 2.73 us
where the time goes in v2:
time: 120 us
  Pallas kernels  118 us (98%)
  local copies, waits for them, and re-layouts  2.73 us (2%)
    pallas_call x1, Pallas kernels, local(): pl.pallas_call(kernel, name='mixer_ffn', out_shape=jax.ShapeDtypeStruct((...  118 us
    unnamed x1, local copies, waits for them, and re-layouts  2.73 us

profile of v2, /device:TPU:0, one launch (start us, length us, event | category | flops | bytes accessed | tf_op | source)
XLA Modules:
  0.0 120.3 jit_solution(8888595935914982681)
XLA Ops:
  0.0 117.5 %mixer_ffn.1 = bf16[384,2048]{1,0:T(8,128)(2,1)} custom-call(bf16[384,2048]{1,0:T(8,128)(2,1)} %tok.1, f32[64,768]{1,0:T(8,128)} %wo_in.1, f32[64,768]{1,0:T(8,128)} %wi_in.1, f32[64,768]{1,0:T(8,128)} %wv_in.1, f32[64,768]{1,0:T(8,128)} %bitcast.5, f32[64,2048]{1,0:T(8,128)} %wu_in.1, f32[64,2048]{1,0:T(8,128)} %bitcast.4, f32[3,768]{1,0:T(4,128)} %taps.1, ...), custom_call_target="tpu_custom_call" | custom-call | tf_op jit(solution)/shard_map/mixer_ffn/pallas_call | solution.py:415
  117.5 2.7 %copy.12 = bf16[384,2048]{1,0:T(8,128)(2,1)} copy(bf16[384,2048]{1,0:T(8,128)(2,1)} %mixer_ffn.1) | data formatting | bytes 3145728

commit v3 on v2

v3 whole, which is shorter than its diff:
```python
import jax
import jax.numpy as jnp
from jax import lax
from jax.experimental import pallas as pl
from jax.experimental.pallas import tpu as pltpu
from jax.sharding import Mesh
from jax.sharding import PartitionSpec as P

SEQ = 128
FS = ("fs_0", "fs_1", "fs_2")
REP_FS_TP = ("rep", "fs_0", "fs_1", "fs_2", "tp")
MESH = pl.DeviceIdType.MESH
SCALE = 2.0**0.25
EPS = 1e-05
F32 = jnp.float32
BF16 = jnp.bfloat16

D = 2048
ROWS = 64
TOK = 384
CH = 384
HID = 1024
NSEQ = TOK // SEQ
WIDTHS = (4 * CH, HID, HID)
MIXER, UP, DOWN = range(3)
COLS = 256
NCOL = D // COLS


def kernel(
    tok, wo_in, wi_in, wv_in, wm_in, wu_in, wd_in, taps, gain1, gain2, out,
    wp, wu, wd, wm2, gp, gu, gd, stage_p, stage_u, stage_d,
    x, f, mixed, mixed2, hid, pd, d_send, d_recv, z_send, z_recv, acc, held,
    s_in, sw_send, sw_recv, sz_send, sz_recv, sx_own, sx_send, sx_recv, sf_send, sf_recv,
    sq_send, sq_recv, sm_send, sm_recv, sd_send, sd_recv, sr_send, sr_recv, s_out,
):
    rep, zl = lax.axis_index("rep"), lax.axis_index("fs_0")
    my_y, my_x, core = lax.axis_index("fs_1"), lax.axis_index("fs_2"), lax.axis_index("tp")
    z = rep * 2 + zl

    def device(z_, y_, x_, c_):
        return (z_ // 2, z_ % 2, y_, x_, c_)

    z_plus, z_minus = (z + 1) % 4, (z + 3) % 4
    above, below = device(z_plus, my_y, my_x, core), device(z_minus, my_y, my_x, core)
    sibling = device(z, my_y, my_x, 1 - core)
    z_to = (z + 3 + 2 * core) % 4
    z_from = (z + 1 + 2 * core) % 4
    helper, helped = device(z_to, my_y, my_x, core), device(z_from, my_y, my_x, core)
    x_plus, x_minus = device(z, my_y, (my_x + 1) % 4, core), device(z, my_y, (my_x + 3) % 4, core)
    y_plus, y_minus = device(z, (my_y + 1) % 4, my_x, core), device(z, (my_y + 3) % 4, my_x, core)

    def remote(src, dst, send_sem, recv_sem, target):
        return pltpu.make_async_remote_copy(
            src_ref=src, dst_ref=dst, send_sem=send_sem, recv_sem=recv_sem, device_id=target, device_id_type=MESH
        )

    weights = (wp, wu, wd)
    given = (gp, gu, gd)
    own_row = (zl * 4 + my_y, my_x)
    other_row = ((1 - zl) * 4 + my_y, my_x)

    def load(which):
        pairs = (
            (wo_in, stage_p.at[0]), (wi_in, stage_p.at[1]), (wv_in, stage_p.at[2]), (wm_in, stage_p.at[3]),
            (wu_in, stage_u), (wd_in, stage_d),
        )
        return pltpu.make_async_copy(*pairs[which], s_in.at[which])

    def cast(t):
        keep, give = weights[t].at[own_row[0], own_row[1]], given[t]
        if t == MIXER:
            for which in range(4):
                load(which).wait()
            pieces = [(i, c0, at + i * width, width) for width, c0, at in ((256, 0, 0), (128, 256, 768)) for i in range(3)]
            for i, c0, at, width in pieces + [(3, 0, 3 * CH, CH)]:
                mine = pl.ds(pl.multiple_of(zl * CH + c0, 128), width)
                theirs = pl.ds(pl.multiple_of((1 - zl) * CH + c0, 128), width)
                keep[:, at:at + width] = stage_p[i, :, mine].astype(BF16)
                give[:, at:at + width] = stage_p[i, :, theirs].astype(BF16)
        else:
            stage = {UP: stage_u, DOWN: stage_d}[t]
            load({UP: 4, DOWN: 5}[t]).wait()
            width = WIDTHS[t]
            keep[...] = stage[:, pl.ds(pl.multiple_of(zl * width, 128), width)].astype(BF16)
            give[...] = stage[:, pl.ds(pl.multiple_of((1 - zl) * width, 128), width)].astype(BF16)

    me = ((my_x, my_y), (my_y, my_x))
    plus = ((x_plus, y_plus), (y_plus, x_plus))
    minus = ((x_minus, y_minus), (y_minus, x_minus))
    SHIFT = (0, 3, 1, 2)
    HALF = ROWS // 2

    def block(color, k1, k2):
        i1, i2 = (me[color][0] + SHIFT[k1]) % 4, (me[color][1] + SHIFT[k2]) % 4
        y_, x_ = (i2, i1) if color == 0 else (i1, i2)
        return (color * 4 + y_, x_)

    def wcopy(t, color, slot, row, start, rows, target):
        part = weights[t].at[row[0], row[1], pl.ds(start, rows)]
        return remote(part, part, sw_send.at[t, int(slot == 0)], sw_recv.at[t, color, slot], target)

    def second_leg(t, color, k):
        row = block(color, k, 0)
        wcopy(t, color, 4 + 4 * k, row, 0, ROWS, plus[color][1]).start()
        wcopy(t, color, 5 + 4 * k, row, 0, ROWS, minus[color][1]).start()

    def arrive(t, color, slot, row, start, rows):
        wcopy(t, color, slot, row, start, rows, plus[color][0]).wait_recv()

    def zcopy(t, half, row, target):
        return remote(
            given[t].at[pl.ds(half * HALF, HALF)], weights[t].at[row[0], row[1], pl.ds(half * HALF, HALF)],
            sz_send.at[t, half], sz_recv.at[t, half], target,
        )

    def start_z(t):
        zcopy(t, 0, own_row, above).start()
        zcopy(t, 1, own_row, below).start()

    def both_legs(t, color, row):
        for slot, step in ((0, 1), (1, 3)):
            wcopy(t, color, slot, row, 0, ROWS, device(z, (my_y + step * color) % 4, (my_x + step * (1 - color)) % 4, core)).start()
        for slot, step in ((4, 1), (5, 3)):
            wcopy(t, color, slot, row, 0, ROWS, device(z, (my_y + step * (1 - color)) % 4, (my_x + step * color) % 4, core)).start()

    def g0_own(t):
        both_legs(t, zl, own_row)

    def g0_other(t):
        zcopy(t, 0, other_row, above).wait_recv()
        zcopy(t, 1, other_row, below).wait_recv()
        both_legs(t, 1 - zl, other_row)

    def g1(t):
        for color in (0, 1):
            row = block(color, 1, 0)
            arrive(t, color, 0, row, 0, ROWS)
            wcopy(t, color, 2, row, 0, HALF, plus[color][0]).start()
        for color in (0, 1):
            row = block(color, 2, 0)
            arrive(t, color, 1, row, 0, ROWS)
            wcopy(t, color, 3, row, HALF, HALF, minus[color][0]).start()
        for color in (0, 1):
            second_leg(t, color, 1)
            second_leg(t, color, 2)

    def g2(t):
        for color in (0, 1):
            row = block(color, 3, 0)
            arrive(t, color, 2, row, 0, HALF)
            arrive(t, color, 3, row, HALF, HALF)
            second_leg(t, color, 3)

    def g3(t, k):
        for color in (0, 1):
            row = block(color, k, 1)
            arrive(t, color, 4 + 4 * k, row, 0, ROWS)
            wcopy(t, color, 6 + 4 * k, row, 0, HALF, plus[color][1]).start()
            row = block(color, k, 2)
            arrive(t, color, 5 + 4 * k, row, 0, ROWS)
            wcopy(t, color, 7 + 4 * k, row, HALF, HALF, minus[color][1]).start()

    def g4(t):
        for k in range(4):
            for color in (0, 1):
                row = block(color, k, 3)
                arrive(t, color, 6 + 4 * k, row, 0, HALF)
                arrive(t, color, 7 + 4 * k, row, HALF, HALF)

    def chunk(color, k):
        return (me[color][1] + SHIFT[k]) % 4

    def chunk_rows(ref, color, at):
        return ref.at[at] if color == 0 else ref.at[pl.ds(4, 4), at]

    def mix_swap(k, color):
        source = chunk_rows(wp, color, chunk(color, k)).at[:, :, pl.ds(3 * CH, CH)]
        return remote(
            source, chunk_rows(wm2, color, chunk(color, k)), sq_send.at[k, color], sq_recv.at[k, color], (above, below)[color]
        )

    def seq(s):
        return pl.ds(s * SEQ, SEQ)

    def tok_z(s):
        return remote(tok.at[seq(s)], x.at[2, seq(s)], sx_send.at[0], sx_recv.at[1 + s], helper)

    def tok_sibling():
        return remote(tok, x.at[1], sx_send.at[1], sx_recv.at[0], sibling)

    def tok_relay(s):
        return remote(x.at[2, seq(s)], x.at[3, seq(s)], sx_send.at[2], sx_recv.at[4 + s], sibling)

    def first_copy(kind, s):
        source, target, to = ((0, 1, sibling), (0, 2, helper), (2, 3, sibling))[kind]
        return remote(f.at[source, seq(s)], f.at[target, seq(s)], sf_send.at[kind], sf_recv.at[kind, s], to)

    def mixed_copy(i):
        return remote(mixed.at[2 + i], mixed2.at[i], sm_send.at[i], sm_recv.at[i], (helped, helper)[i])

    def part_copy(phase, slot, i, j):
        return remote(d_send.at[slot, j], d_recv.at[slot, j], sd_send.at[phase, slot], sd_recv.at[phase, slot, i], sibling)

    def sum_copy(k, color):
        j = color * 4 + chunk(color, k)
        return remote(z_send.at[j], z_recv.at[j], sr_send, sr_recv.at[k * 2 + color], helped)

    def relay_tokens(s):
        tok_z(s).wait_recv()
        tok_relay(s).start()

    def all_sent(ref, sem):
        remote(ref, ref, sem, sw_recv.at[0, 0, 0], x_plus).wait_send()

    row_id = lax.broadcasted_iota(jnp.int32, (SEQ, 1), 0)

    def convolve(g, ch, c0):
        tap = [taps[k:k + 1, pl.ds(pl.multiple_of(zl * CH + c0, 128), ch)] for k in range(3)]
        for s in range(NSEQ):
            rows = pl.ds(s * SEQ, SEQ)
            product = pd[rows, pl.ds(ch, ch)] * pd[rows, pl.ds(2 * ch, ch)]
            before = jnp.where(row_id > 0, pltpu.roll(product, 1, 0), 0.0)
            after = jnp.where(row_id < SEQ - 1, pltpu.roll(product, SEQ - 1, 0), 0.0)
            conv = tap[0] * before + tap[1] * product + tap[2] * after
            mixed[g, rows, c0:c0 + ch] = (pd[rows, pl.ds(0, ch)] * conv).astype(BF16)

    def project(g):
        pd[...] = jnp.dot(x[g], wp[:, :, :, 0:768].reshape(D, 768), preferred_element_type=F32)
        convolve(g, 256, 0)
        pd[:, 0:384] = jnp.dot(x[g], wp[:, :, :, 768:1152].reshape(D, 384), preferred_element_type=F32)
        convolve(g, 128, 256)

    def dot_t(rows, w):
        return lax.dot_general(
            rows, w.reshape(COLS, w.shape[-1]), (((1,), (1,)), ((), ())), preferred_element_type=F32
        )

    def pair(ref, g):
        return ref[g:g + 2].reshape(2 * TOK, ref.shape[-1])

    def mix_sums(j):
        total = dot_t(pair(mixed, 0), wp[j, :, :, 3 * CH:4 * CH]) + dot_t(pair(mixed2, 0), wm2[j])
        acc[j] = total[:TOK]
        d_send[0, j] = total[TOK:].astype(BF16)
        part_copy(0, 0, j, j).start()

    def ffn_sums(g, k, color):
        j = color * 4 + chunk(color, k)
        slot = g // 2
        w = wd[j] if color == 0 else wd[4:8, j - 4]
        total = dot_t(pair(hid, g), w)
        d_send[slot, j] = total[TOK:].astype(BF16)
        part_copy(1, slot, k * 2 + color, j).start()
        if g == 0:
            acc[j] = total[:TOK]
        else:
            held[k % 2, color] = total[:TOK]

    def ffn_send(k, color):
        j = color * 4 + chunk(color, k)
        part_copy(1, 1, k * 2 + color, j).wait_recv()
        z_send[j] = (held[k % 2, color] + d_recv[1, j].astype(F32)).astype(BF16)
        sum_copy(k, color).start()

    low = lax.broadcasted_iota(jnp.int32, (1, 128), 1) < 64

    def natural(parts):
        tiles = [[parts[4 + x_][:, q * 128:(q + 1) * 128] for q in (0, 1)] for x_ in range(4)]
        result = list(parts[:4])
        for y_ in range(4):
            for p in (0, 1):
                a, b = tiles[2 * p][y_ // 2], tiles[2 * p + 1][y_ // 2]
                if y_ % 2 == 0:
                    result.append(jnp.where(low, a, pltpu.roll(b, 64, 1)))
                else:
                    result.append(jnp.where(low, pltpu.roll(a, 64, 1), b))
        return jnp.concatenate(result, axis=1)

    def normed(base, arrived, gain, s, target):
        step_rows = 32

        def step(i, _):
            rows = pl.ds(pl.multiple_of(s * SEQ + i * step_rows, step_rows), step_rows)
            v = SCALE * base[0, rows, :].astype(F32) + arrived(rows)
            center = v - jnp.mean(v, axis=-1, keepdims=True)
            spread = jnp.mean(center * center, axis=-1, keepdims=True)
            target[0, rows, :] = (center * lax.rsqrt(spread + EPS) * gain[...]).astype(BF16)
            return 0

        lax.fori_loop(0, SEQ // step_rows, step, 0)

    def expand(g, s=None):
        rows = pl.ds(0, TOK) if s is None else seq(s)

        def step(j, _):
            cols = pl.ds(pl.multiple_of(j * 512, 512), 512)
            raised = jnp.maximum(jnp.dot(f[g, rows, :], wu[:, :, :, cols].reshape(D, 512), preferred_element_type=F32), 0.0)
            hid[g, rows, cols] = (raised * raised).astype(BF16)
            return 0

        lax.fori_loop(0, HID // 512, step, 0)

    barrier = pltpu.get_barrier_semaphore()
    for other in (x_plus, x_minus, y_plus, y_minus, above, below, sibling):
        pl.semaphore_signal(barrier, inc=1, device_id=other, device_id_type=MESH)
    own_tokens = pltpu.make_async_copy(tok, x.at[0], sx_own)
    for which in range(6):
        load(which).start()
    own_tokens.start()
    for t in range(3):
        cast(t)
    pl.semaphore_wait(barrier, 7)

    start_z(MIXER)
    g0_own(MIXER)
    tok_z(0).start()
    tok_sibling().start()
    start_z(UP)
    tok_z(1).start()
    tok_z(2).start()
    start_z(DOWN)
    g0_other(MIXER)
    g1(MIXER)
    g3(MIXER, 0)
    relay_tokens(0)
    g2(MIXER)
    for color in (0, 1):
        mix_swap(0, color).start()
    g3(MIXER, 1)
    relay_tokens(1)
    g3(MIXER, 2)
    relay_tokens(2)
    g3(MIXER, 3)
    for k in (1, 2):
        for color in (0, 1):
            mix_swap(k, color).start()
    g0_own(UP)
    g0_other(UP)
    for s in range(NSEQ):
        tok_relay(s).wait_recv()
    tok_sibling().wait_recv()
    own_tokens.wait()
    g4(MIXER)
    for color in (0, 1):
        mix_swap(3, color).start()
    project(3)
    mixed_copy(1).start()
    g1(UP)
    g3(UP, 0)
    project(2)
    mixed_copy(0).start()
    g2(UP)
    g3(UP, 1)
    project(1)
    g3(UP, 2)
    g3(UP, 3)
    g0_own(DOWN)
    g0_other(DOWN)
    project(0)
    for k in range(4):
        for color in (0, 1):
            mix_swap(k, color).wait_recv()
    mixed_copy(1).wait_recv()
    mixed_copy(0).wait_recv()
    for j in range(NCOL):
        mix_sums(j)
    for j in range(NCOL):
        part_copy(0, 0, j, j).wait_recv()

    def mixing(rows):
        return jnp.concatenate([acc[j, rows, :] + d_recv[0, j, rows, :].astype(F32) for j in range(NCOL)], axis=1)

    for s in range(NSEQ):
        normed(x, mixing, gain1, s, f)
        first_copy(1, s).start()
        first_copy(0, s).start()
    g4(UP)
    g1(DOWN)
    g3(DOWN, 0)
    expand(0)
    g2(DOWN)
    for s in range(NSEQ):
        first_copy(0, s).wait_recv()
    expand(1)
    g3(DOWN, 1)
    all_sent(d_send.at[0], sd_send.at[0, 0])
    for s in range(NSEQ):
        first_copy(1, s).wait_recv()
        first_copy(2, s).start()
        expand(2, s)
        if s == 0:
            g3(DOWN, 2)
        if s == 1:
            g3(DOWN, 3)
        first_copy(2, s).wait_recv()
        expand(3, s)
    pieces = [(k, color) for k in range(4) for color in (0, 1)]
    for n, (k, color) in enumerate(pieces):
        if n == 6:
            ffn_sums(0, 0, 0)
            ffn_sums(0, 0, 1)
            g4(DOWN)
        ffn_sums(2, k, color)
        if n in (0, 6):
            continue
        ffn_send(*pieces[n - 1])
        if n == 5:
            ffn_send(*pieces[5])
    ffn_send(*pieces[7])
    for k in (1, 2, 3):
        for color in (0, 1):
            ffn_sums(0, k, color)
    for k, color in pieces:
        part_copy(1, 0, k * 2 + color, color * 4 + chunk(color, k)).wait_recv()
        sum_copy(k, color).wait_recv()

    def lowered(rows):
        return natural([
            acc[j, rows, :] + d_recv[0, j, rows, :].astype(F32) + z_recv[j, rows, :].astype(F32) for j in range(NCOL)
        ])

    results = []
    for s in range(NSEQ):
        normed(f, lowered, gain2, s, x)
        results.append(pltpu.make_async_copy(x.at[0, seq(s)], out.at[seq(s)], s_out.at[s]))
        results[-1].start()

    for t in range(3):
        all_sent(weights[t].at[pl.ds(0, 7)], sw_send.at[t, 0])
        all_sent(weights[t].at[0, pl.ds(0, 2)], sw_send.at[t, 1])
        zcopy(t, 0, own_row, above).wait_send()
        zcopy(t, 1, own_row, below).wait_send()
    for kind in range(3):
        all_sent(x.at[0], sx_send.at[kind])
        all_sent(f.at[0], sf_send.at[kind])
    for k in range(4):
        for color in (0, 1):
            mix_swap(k, color).wait_send()
    for i in (0, 1):
        mixed_copy(i).wait_send()
        all_sent(d_send.at[i], sd_send.at[1, i])
    all_sent(z_send, sr_send)
    for result in results:
        result.wait()


def local(tokens, outer_weight, inner_weight, value_weight, conv_taps, mix_out, norm_first, up_weight, down_weight, norm_second):
    hbm = pl.BlockSpec(memory_space=pl.ANY)
    vmem = pl.BlockSpec(memory_space=pltpu.VMEM)
    dma = pltpu.SemaphoreType.DMA
    return pl.pallas_call(
        kernel,
        name="mixer_ffn",
        out_shape=jax.ShapeDtypeStruct((TOK, D), BF16),
        in_specs=[hbm] * 7 + [vmem] * 3,
        out_specs=hbm,
        scratch_shapes=[pltpu.VMEM((8, 4, ROWS, w), BF16) for w in WIDTHS]
        + [pltpu.VMEM((8, 4, ROWS, CH), BF16)]
        + [pltpu.VMEM((ROWS, w), BF16) for w in WIDTHS]
        + [
            pltpu.VMEM((4, ROWS, 2 * CH), F32),
            pltpu.VMEM((ROWS, 2 * HID), F32),
            pltpu.VMEM((ROWS, 2 * HID), F32),
            pltpu.VMEM((4, TOK, D), BF16),
            pltpu.VMEM((4, TOK, D), BF16),
            pltpu.VMEM((4, TOK, CH), BF16),
            pltpu.VMEM((2, TOK, CH), BF16),
            pltpu.VMEM((4, TOK, HID), BF16),
            pltpu.VMEM((TOK, 768), F32),
            pltpu.VMEM((2, NCOL, TOK, COLS), BF16),
            pltpu.VMEM((2, NCOL, TOK, COLS), BF16),
            pltpu.VMEM((NCOL, TOK, COLS), BF16),
            pltpu.VMEM((NCOL, TOK, COLS), BF16),
            pltpu.VMEM((NCOL, TOK, COLS), F32),
            pltpu.VMEM((2, 2, TOK, COLS), F32),
            dma((6,)),
            dma((3, 2)),
            dma((3, 2, 20)),
            dma((3, 2)),
            dma((3, 2)),
            dma,
            dma((3,)),
            dma((7,)),
            dma((3,)),
            dma((3, 3)),
            dma((4, 2)),
            dma((4, 2)),
            dma((2,)),
            dma((2,)),
            dma((2, 2)),
            dma((2, 2, 8)),
            dma,
            dma((8,)),
            dma((3,)),
        ],
        compiler_params=pltpu.CompilerParams(
            collective_id=0, has_side_effects=True, vmem_limit_bytes=62 * 1024 * 1024
        ),
    )(
        tokens, outer_weight, inner_weight, value_weight, mix_out.T, up_weight, down_weight.T,
        conv_taps, norm_first.reshape(1, D), norm_second.reshape(1, D),
    )


def solution(mesh):
    finer = Mesh(
        mesh.devices.reshape(mesh.shape["rep"], 2, 4, 4, mesh.shape["tp"]),
        ("rep", "fs_0", "fs_1", "fs_2", "tp"),
    )
    placed = (
        P(REP_FS_TP, None),
        P(FS, "tp"),
        P(FS, "tp"),
        P(FS, "tp"),
        P(None, "tp"),
        P("tp", FS),
        P(),
        P(FS, "tp"),
        P("tp", FS),
        P(),
    )
    return jax.shard_map(
        local, mesh=finer, in_specs=placed, out_specs=P(REP_FS_TP, None), check_vma=False
    )
```

time: 120 us -> 128 us (1.067)
  Pallas kernels: 118 us -> 125 us
    pallas_call x1, Pallas kernels: 118 us -> 125 us  [local(): pl.pallas_call(kernel, name='mixer_ffn', out_shape=jax.ShapeDtypeStruct((...]
where the time goes in v3:
time: 128 us
  Pallas kernels  125 us (98%)
  local copies, waits for them, and re-layouts  2.73 us (2%)
    pallas_call x1, Pallas kernels, local(): pl.pallas_call(kernel, name='mixer_ffn', out_shape=jax.ShapeDtypeStruct((...  125 us
    unnamed x1, local copies, waits for them, and re-layouts  2.73 us

profile of v3, /device:TPU:0, one launch (start us, length us, event | category | flops | bytes accessed | tf_op | source)
XLA Modules:
  0.0 128.0 jit_solution(13547953254469712319)
XLA Ops:
  0.0 125.3 %mixer_ffn.1 = bf16[384,2048]{1,0:T(8,128)(2,1)} custom-call(bf16[384,2048]{1,0:T(8,128)(2,1)} %tok.1, f32[64,768]{1,0:T(8,128)} %wo_in.1, f32[64,768]{1,0:T(8,128)} %wi_in.1, f32[64,768]{1,0:T(8,128)} %wv_in.1, f32[64,768]{1,0:T(8,128)} %bitcast.5, f32[64,2048]{1,0:T(8,128)} %wu_in.1, f32[64,2048]{1,0:T(8,128)} %bitcast.4, f32[3,768]{1,0:T(4,128)} %taps.1, ...), custom_call_target="tpu_custom_call" | custom-call | tf_op jit(solution)/shard_map/mixer_ffn/pallas_call | solution.py:452
  125.3 2.7 %copy.12 = bf16[384,2048]{1,0:T(8,128)(2,1)} copy(bf16[384,2048]{1,0:T(8,128)(2,1)} %mixer_ffn.1) | data formatting | bytes 3145728

commit v4 on v3

v4 whole, which is shorter than its diff:
```python
import jax
import jax.numpy as jnp
from jax import lax
from jax.experimental import pallas as pl
from jax.experimental.pallas import tpu as pltpu
from jax.sharding import Mesh
from jax.sharding import PartitionSpec as P

SEQ = 128
FS = ("fs_0", "fs_1", "fs_2")
REP_FS_TP = ("rep", "fs_0", "fs_1", "fs_2", "tp")
MESH = pl.DeviceIdType.MESH
SCALE = 2.0**0.25
EPS = 1e-05
F32 = jnp.float32
BF16 = jnp.bfloat16

D = 2048
ROWS = 64
TOK = 384
CH = 384
HID = 1024
NSEQ = TOK // SEQ
WIDTHS = (4 * CH, HID, HID)
MIXER, UP, DOWN = range(3)
COLS = 256
NCOL = D // COLS


def kernel(
    tok, wo_in, wi_in, wv_in, wm_in, wu_in, wd_in, taps, gain1, gain2, out,
    wp, wu, wd, wm2, gp, gu, gd,
    own, x, f, mixed, mixed2, hid, pd, d_send, d_recv, z_send, z_recv, acc, held,
    s_in, sw_send, sw_recv, sz_send, sz_recv, sx_own, sx_send, sx_recv, sf_send, sf_recv,
    sq_send, sq_recv, sm_send, sm_recv, sd_send, sd_recv, sr_send, sr_recv, s_out,
):
    rep, zl = lax.axis_index("rep"), lax.axis_index("fs_0")
    my_y, my_x, core = lax.axis_index("fs_1"), lax.axis_index("fs_2"), lax.axis_index("tp")
    z = rep * 2 + zl

    def device(z_, y_, x_, c_):
        return (z_ // 2, z_ % 2, y_, x_, c_)

    z_plus, z_minus = (z + 1) % 4, (z + 3) % 4
    above, below = device(z_plus, my_y, my_x, core), device(z_minus, my_y, my_x, core)
    sibling = device(z, my_y, my_x, 1 - core)
    z_to = (z + 3 + 2 * core) % 4
    z_from = (z + 1 + 2 * core) % 4
    helper, helped = device(z_to, my_y, my_x, core), device(z_from, my_y, my_x, core)
    x_plus, x_minus = device(z, my_y, (my_x + 1) % 4, core), device(z, my_y, (my_x + 3) % 4, core)
    y_plus, y_minus = device(z, (my_y + 1) % 4, my_x, core), device(z, (my_y + 3) % 4, my_x, core)

    def remote(src, dst, send_sem, recv_sem, target):
        return pltpu.make_async_remote_copy(
            src_ref=src, dst_ref=dst, send_sem=send_sem, recv_sem=recv_sem, device_id=target, device_id_type=MESH
        )

    weights = (wp, wu, wd)
    given = (gp, gu, gd)
    own_row = (zl * 4 + my_y, my_x)
    other_row = ((1 - zl) * 4 + my_y, my_x)

    def stage(which, width):
        return pd.at[pl.ds(pl.multiple_of(which * ROWS, ROWS), ROWS), pl.ds(0, width)]

    def load(which):
        if which < 4:
            source = (wo_in, wi_in, wv_in, wm_in)[which]
        else:
            source = (wu_in, wd_in)[which // 2 - 2].at[:, pl.ds(which % 2 * HID, HID)]
        return pltpu.make_async_copy(source, stage(which, 2 * CH if which < 4 else HID), s_in.at[which])

    def cast(t):
        keep, give = weights[t].at[own_row[0], own_row[1]], given[t]
        if t == MIXER:
            for which in range(4):
                load(which).wait()
            pieces = [(i, c0, at + i * width, width) for width, c0, at in ((256, 0, 0), (128, 256, 768)) for i in range(3)]
            for i, c0, at, width in pieces + [(3, 0, 3 * CH, CH)]:
                kept = pl.ds(pl.multiple_of(zl * CH + c0, 128), width)
                passed = pl.ds(pl.multiple_of((1 - zl) * CH + c0, 128), width)
                keep[:, at:at + width] = pd[i * ROWS:(i + 1) * ROWS, kept].astype(BF16)
                give[:, at:at + width] = pd[i * ROWS:(i + 1) * ROWS, passed].astype(BF16)
        else:
            first = 2 + 2 * t
            load(first).wait()
            load(first + 1).wait()
            keep[...] = stage(first + zl, HID)[...].astype(BF16)
            give[...] = stage(first + 1 - zl, HID)[...].astype(BF16)

    SHIFT = (0, 3, 1, 2)
    HALF = ROWS // 2
    mine, theirs = zl, 1 - zl

    def block(color, k1, k2):
        y_ = (my_y + SHIFT[k1] * color + SHIFT[k2] * (1 - color)) % 4
        x_ = (my_x + SHIFT[k1] * (1 - color) + SHIFT[k2] * color) % 4
        return (color * 4 + y_, x_)

    def ring(color, leg, step):
        along_y = color if leg == 1 else 1 - color
        return device(z, (my_y + step * along_y) % 4, (my_x + step * (1 - along_y)) % 4, core)

    def wcopy(t, color, slot, row, start, rows, target):
        part = weights[t].at[row[0], row[1], pl.ds(start, rows)]
        return remote(part, part, sw_send.at[t, int(slot == 0)], sw_recv.at[t, color, slot], target)

    def arrive(t, color, slot, row, start, rows):
        wcopy(t, color, slot, row, start, rows, x_plus).wait_recv()

    def first_leg(t, color):
        row = block(color, 0, 0)
        wcopy(t, color, 0, row, 0, ROWS, ring(color, 1, 1)).start()
        wcopy(t, color, 1, row, 0, ROWS, ring(color, 1, 3)).start()

    def second_leg(t, color, k):
        row = block(color, k, 0)
        wcopy(t, color, 4 + 4 * k, row, 0, ROWS, ring(color, 2, 1)).start()
        wcopy(t, color, 5 + 4 * k, row, 0, ROWS, ring(color, 2, 3)).start()

    def zcopy(t, half, row, target):
        return remote(
            given[t].at[pl.ds(half * HALF, HALF)], weights[t].at[row[0], row[1], pl.ds(half * HALF, HALF)],
            sz_send.at[t, half], sz_recv.at[t, half], target,
        )

    def start_z(t):
        zcopy(t, 0, own_row, above).start()
        zcopy(t, 1, own_row, below).start()

    def z_arrived(t):
        zcopy(t, 0, other_row, above).wait_recv()
        zcopy(t, 1, other_row, below).wait_recv()

    def g1(t, color):
        row = block(color, 1, 0)
        arrive(t, color, 0, row, 0, ROWS)
        wcopy(t, color, 2, row, 0, HALF, ring(color, 1, 1)).start()
        row = block(color, 2, 0)
        arrive(t, color, 1, row, 0, ROWS)
        wcopy(t, color, 3, row, HALF, HALF, ring(color, 1, 3)).start()

    def g2(t, color):
        row = block(color, 3, 0)
        arrive(t, color, 2, row, 0, HALF)
        arrive(t, color, 3, row, HALF, HALF)

    def g3(t, color, k):
        row = block(color, k, 1)
        arrive(t, color, 4 + 4 * k, row, 0, ROWS)
        wcopy(t, color, 6 + 4 * k, row, 0, HALF, ring(color, 2, 1)).start()
        row = block(color, k, 2)
        arrive(t, color, 5 + 4 * k, row, 0, ROWS)
        wcopy(t, color, 7 + 4 * k, row, HALF, HALF, ring(color, 2, 3)).start()

    def g4(t):
        for k in range(4):
            for color in (mine, theirs):
                row = block(color, k, 3)
                arrive(t, color, 6 + 4 * k, row, 0, HALF)
                arrive(t, color, 7 + 4 * k, row, HALF, HALF)

    def chunk(color, k):
        return ((my_y, my_x)[color] + SHIFT[k]) % 4

    def chunk_rows(ref, color, at):
        return ref.at[at] if color == 0 else ref.at[pl.ds(4, 4), at]

    def mix_swap(k, color):
        source = chunk_rows(wp, color, chunk(color, k)).at[:, :, pl.ds(3 * CH, CH)]
        return remote(
            source, chunk_rows(wm2, color, chunk(color, k)), sq_send.at[k, color], sq_recv.at[k, color], (above, below)[color]
        )

    def seq(s):
        return pl.ds(s * SEQ, SEQ)

    def tok_z(s):
        return remote(x.at[0, :, seq(s)], x.at[2, :, seq(s)], sx_send.at[0], sx_recv.at[1 + s], helper)

    def tok_sibling():
        return remote(x.at[0], x.at[1], sx_send.at[1], sx_recv.at[0], sibling)

    def tok_relay(s):
        return remote(x.at[2, :, seq(s)], x.at[3, :, seq(s)], sx_send.at[2], sx_recv.at[4 + s], sibling)

    def first_copy(kind, s):
        source, target, to = ((0, 1, sibling), (0, 2, helper), (2, 3, sibling))[kind]
        return remote(f.at[source, seq(s)], f.at[target, seq(s)], sf_send.at[kind], sf_recv.at[kind, s], to)

    def mixed_copy(i):
        return remote(mixed.at[2 + i], mixed2.at[i], sm_send.at[i], sm_recv.at[i], (helped, helper)[i])

    def mix_copy(s):
        rows = (0, slice(None), seq(s))
        return remote(d_send.at[rows], d_recv.at[rows], sd_send.at[0, 0], sd_recv.at[0, 0, s], sibling)

    def piece(k, color, s):
        j = color * 4 + chunk(color, k)
        return j, pl.ds(0, TOK) if s is None else seq(s), (k * 2 + color) * NSEQ + (s or 0)

    def part_copy(slot, k, color, s=None):
        j, rows, at = piece(k, color, s)
        return remote(d_send.at[slot, j, rows], d_recv.at[slot, j, rows], sd_send.at[1, slot], sd_recv.at[1, slot, at], sibling)

    def sum_copy(k, color, s=None):
        j, rows, at = piece(k, color, s)
        return remote(z_send.at[j, rows], z_recv.at[j, rows], sr_send, sr_recv.at[at], helped)

    def relay_tokens(s):
        tok_z(s).wait_recv()
        tok_relay(s).start()

    def all_sent(ref, sem):
        remote(ref, ref, sem, sw_recv.at[0, 0, 0], x_plus).wait_send()

    row_id = lax.broadcasted_iota(jnp.int32, (SEQ, 1), 0)

    low = lax.broadcasted_iota(jnp.int32, (1, 128), 1) < 64

    def spread_tokens():
        for j in range(4):
            x[0, j] = own[:, j * COLS:(j + 1) * COLS]
        for x_ in range(4):
            for q in (0, 1):
                a, b = (
                    own[:, pl.ds(1024 + y_ * COLS + (x_ // 2) * 128, 128)].astype(F32) for y_ in (2 * q, 2 * q + 1)
                )
                if x_ % 2 == 0:
                    joined = jnp.where(low, a, pltpu.roll(b, 64, 1))
                else:
                    joined = jnp.where(low, pltpu.roll(a, 64, 1), b)
                x[0, 4 + x_, :, q * 128:(q + 1) * 128] = joined.astype(BF16)

    def project(p, k):
        rows = pl.ds(p * 2 * TOK, 2 * TOK)
        j0, j1 = chunk(0, k), chunk(1, k)
        for a, b in ((0, 768), (768, 1152)):
            total = jnp.dot(
                x[2 * p:2 * p + 2, j0].reshape(2 * TOK, COLS), wp[j0, :, :, a:b].reshape(COLS, b - a),
                preferred_element_type=F32,
            ) + jnp.dot(
                x[2 * p:2 * p + 2, 4 + j1].reshape(2 * TOK, COLS), wp[4:8, j1, :, a:b].reshape(COLS, b - a),
                preferred_element_type=F32,
            )
            if k == 0:
                pd[rows, a:b] = total
            else:
                pd[rows, a:b] += total

    def convolve(g):
        for ch, c0, at in ((256, 0, 0), (128, 256, 768)):
            tap = [taps[k:k + 1, pl.ds(pl.multiple_of(zl * CH + c0, 128), ch)] for k in range(3)]
            for s in range(NSEQ):
                rows = pl.ds(g * TOK + s * SEQ, SEQ)
                product = pd[rows, pl.ds(at + ch, ch)] * pd[rows, pl.ds(at + 2 * ch, ch)]
                before = jnp.where(row_id > 0, pltpu.roll(product, 1, 0), 0.0)
                after = jnp.where(row_id < SEQ - 1, pltpu.roll(product, SEQ - 1, 0), 0.0)
                conv = tap[0] * before + tap[1] * product + tap[2] * after
                mixed[g, seq(s), c0:c0 + ch] = (pd[rows, pl.ds(at, ch)] * conv).astype(BF16)

    def dot_t(rows, w):
        return lax.dot_general(
            rows, w.reshape(COLS, w.shape[-1]), (((1,), (1,)), ((), ())), preferred_element_type=F32
        )

    def mix_sums(s):
        rows = seq(s)
        left, right = mixed[0:2, rows, :].reshape(2 * SEQ, CH), mixed2[0:2, rows, :].reshape(2 * SEQ, CH)
        for j in range(NCOL):
            total = dot_t(left, wp[j, :, :, 3 * CH:4 * CH]) + dot_t(right, wm2[j])
            acc[j, rows, :] = total[:SEQ]
            d_send[0, j, rows, :] = total[SEQ:].astype(BF16)
        mix_copy(s).start()

    def ffn_sums(p, k, s=None):
        rows = pl.ds(0, TOK) if s is None else seq(s)
        half = TOK if s is None else SEQ
        for color in (0, 1):
            j = color * 4 + chunk(color, k)
            w = wd[j] if color == 0 else wd[4:8, j - 4]
            total = dot_t(hid[2 * p:2 * p + 2, rows, :].reshape(2 * half, HID), w)
            d_send[p, j, rows, :] = total[half:].astype(BF16)
            if p == 0:
                acc[j, rows, :] = total[:half]
            else:
                held[k % 2, color, rows, :] = total[:half]
        for color in (0, 1):
            part_copy(p, k, color, s).start()

    def ffn_send(k, s=None):
        for color in (0, 1):
            if k < 3:
                part_copy(1, k, color, s).wait_recv()
        for color in (0, 1):
            j, rows, _ = piece(k, color, s)
            z_send[j, rows, :] = (held[k % 2, color, rows, :] + d_recv[1, j, rows, :].astype(F32)).astype(BF16)
        for color in (0, 1):
            sum_copy(k, color, s).start()

    def natural(parts):
        tiles = [[parts[4 + x_][:, q * 128:(q + 1) * 128] for q in (0, 1)] for x_ in range(4)]
        result = list(parts[:4])
        for y_ in range(4):
            for p in (0, 1):
                a, b = tiles[2 * p][y_ // 2], tiles[2 * p + 1][y_ // 2]
                if y_ % 2 == 0:
                    result.append(jnp.where(low, a, pltpu.roll(b, 64, 1)))
                else:
                    result.append(jnp.where(low, pltpu.roll(a, 64, 1), b))
        return jnp.concatenate(result, axis=1)

    def normed(base, arrived, gain, s, target):
        step_rows = 32

        def step(i, _):
            rows = pl.ds(pl.multiple_of(s * SEQ + i * step_rows, step_rows), step_rows)
            v = SCALE * base[rows, :].astype(F32) + arrived(rows)
            center = v - jnp.mean(v, axis=-1, keepdims=True)
            spread = jnp.mean(center * center, axis=-1, keepdims=True)
            target[rows, :] = (center * lax.rsqrt(spread + EPS) * gain[...]).astype(BF16)
            return 0

        lax.fori_loop(0, SEQ // step_rows, step, 0)

    def expand(g, s=None):
        rows = pl.ds(0, TOK) if s is None else seq(s)

        def step(j, _):
            cols = pl.ds(pl.multiple_of(j * 512, 512), 512)
            raised = jnp.maximum(jnp.dot(f[g, rows, :], wu[:, :, :, cols].reshape(D, 512), preferred_element_type=F32), 0.0)
            hid[g, rows, cols] = (raised * raised).astype(BF16)
            return 0

        lax.fori_loop(0, HID // 512, step, 0)

    barrier = pltpu.get_barrier_semaphore()
    for other in (x_plus, x_minus, y_plus, y_minus, above, below, sibling):
        pl.semaphore_signal(barrier, inc=1, device_id=other, device_id_type=MESH)
    own_tokens = pltpu.make_async_copy(tok, own, sx_own)
    for which in range(4):
        load(which).start()
    own_tokens.start()
    for which in range(4, 8):
        load(which).start()
    cast(MIXER)
    own_tokens.wait()
    spread_tokens()
    cast(UP)
    cast(DOWN)
    pl.semaphore_wait(barrier, 7)

    both = (mine, theirs)

    def each(step, t, *rest):
        for color in both:
            step(t, color, *rest)

    start_z(MIXER)
    first_leg(MIXER, mine)
    second_leg(MIXER, mine, 0)
    tok_z(0).start()
    tok_sibling().start()
    start_z(UP)
    tok_z(1).start()
    tok_z(2).start()
    start_z(DOWN)
    z_arrived(MIXER)
    first_leg(MIXER, theirs)
    second_leg(MIXER, theirs, 0)
    g1(MIXER, mine)
    second_leg(MIXER, mine, 1)
    relay_tokens(0)
    g1(MIXER, theirs)
    second_leg(MIXER, mine, 2)
    second_leg(MIXER, theirs, 1)
    second_leg(MIXER, theirs, 2)
    g2(MIXER, mine)
    second_leg(MIXER, mine, 3)
    g2(MIXER, theirs)
    second_leg(MIXER, theirs, 3)
    for color in (0, 1):
        mix_swap(0, color).start()
    each(g3, MIXER, 0)
    relay_tokens(1)
    tok_sibling().wait_recv()
    project(0, 0)
    each(g3, MIXER, 1)
    relay_tokens(2)
    each(g3, MIXER, 2)
    for s in range(NSEQ):
        tok_relay(s).wait_recv()
    project(1, 0)
    each(g3, MIXER, 3)
    z_arrived(UP)
    each(first_leg, UP)
    each(second_leg, UP, 0)
    for k in (1, 2):
        for color in (0, 1):
            mix_swap(k, color).start()
    project(1, 1)
    project(1, 2)
    g4(MIXER)
    for color in (0, 1):
        mix_swap(3, color).start()
    project(1, 3)
    convolve(3)
    mixed_copy(1).start()
    convolve(2)
    mixed_copy(0).start()
    each(g1, UP)
    each(second_leg, UP, 1)
    z_arrived(DOWN)
    each(first_leg, DOWN)
    each(second_leg, UP, 2)
    project(0, 1)
    each(g3, UP, 0)
    project(0, 2)
    each(g2, UP)
    each(second_leg, UP, 3)
    project(0, 3)
    convolve(1)
    convolve(0)
    each(g1, DOWN)
    each(g3, UP, 1)
    for k in range(4):
        for color in (0, 1):
            mix_swap(k, color).wait_recv()
    mixed_copy(1).wait_recv()
    mixed_copy(0).wait_recv()

    def mixing(rows):
        return jnp.concatenate([acc[j, rows, :] + d_recv[0, j, rows, :].astype(F32) for j in range(NCOL)], axis=1)

    def make_first(s):
        mix_copy(s).wait_recv()
        normed(own, mixing, gain1, s, f.at[0])
        first_copy(1, s).start()
        first_copy(0, s).start()

    mix_sums(0)
    each(g3, UP, 2)
    mix_sums(1)
    make_first(0)
    mix_sums(2)
    each(g3, UP, 3)
    for k in (0, 1, 2):
        each(second_leg, DOWN, k)
    make_first(1)
    make_first(2)
    each(g2, DOWN)
    each(second_leg, DOWN, 3)
    g4(UP)
    expand(0)
    each(g3, DOWN, 0)
    for s in range(NSEQ):
        first_copy(0, s).wait_recv()
    expand(1)
    all_sent(d_send.at[0], sd_send.at[0, 0])
    for s in range(NSEQ):
        first_copy(1, s).wait_recv()
        first_copy(2, s).start()
        expand(2, s)
        if s > 0:
            ffn_send(0, s - 1)
        first_copy(2, s).wait_recv()
        expand(3, s)
        ffn_sums(1, 0, s)
        each(g3, DOWN, s + 1)
    ffn_sums(1, 1)
    ffn_send(0, 2)
    ffn_sums(1, 2)
    ffn_send(1)
    ffn_sums(0, 0)
    ffn_send(2)
    g4(DOWN)
    ffn_sums(1, 3)
    ffn_sums(0, 1)
    for color in (0, 1):
        part_copy(1, 3, color).wait_recv()
    for s in range(NSEQ):
        ffn_send(3, s)
    ffn_sums(0, 2)
    ffn_sums(0, 3)
    for k in range(4):
        for color in (0, 1):
            part_copy(0, k, color).wait_recv()
            if k == 0:
                for s in range(NSEQ):
                    sum_copy(k, color, s).wait_recv()
            elif k < 3:
                sum_copy(k, color).wait_recv()

    def lowered(rows):
        return natural([
            acc[j, rows, :] + d_recv[0, j, rows, :].astype(F32) + z_recv[j, rows, :].astype(F32) for j in range(NCOL)
        ])

    results = []
    for s in range(NSEQ):
        for color in (0, 1):
            sum_copy(3, color, s).wait_recv()
        normed(f.at[0], lowered, gain2, s, own)
        results.append(pltpu.make_async_copy(own.at[seq(s)], out.at[seq(s)], s_out.at[s]))
        results[-1].start()

    for t in range(3):
        all_sent(weights[t].at[pl.ds(0, 7)], sw_send.at[t, 0])
        all_sent(weights[t].at[0, pl.ds(0, 2)], sw_send.at[t, 1])
        zcopy(t, 0, own_row, above).wait_send()
        zcopy(t, 1, own_row, below).wait_send()
    for kind in range(3):
        all_sent(x.at[0], sx_send.at[kind])
        all_sent(f.at[0], sf_send.at[kind])
    for k in range(4):
        for color in (0, 1):
            mix_swap(k, color).wait_send()
    for i in (0, 1):
        mixed_copy(i).wait_send()
        all_sent(d_send.at[i], sd_send.at[1, i])
    all_sent(z_send, sr_send)
    for result in results:
        result.wait()


def local(tokens, outer_weight, inner_weight, value_weight, conv_taps, mix_out, norm_first, up_weight, down_weight, norm_second):
    hbm = pl.BlockSpec(memory_space=pl.ANY)
    vmem = pl.BlockSpec(memory_space=pltpu.VMEM)
    dma = pltpu.SemaphoreType.DMA
    return pl.pallas_call(
        kernel,
        name="mixer_ffn",
        out_shape=jax.ShapeDtypeStruct((TOK, D), BF16),
        in_specs=[hbm] * 7 + [vmem] * 3,
        out_specs=hbm,
        scratch_shapes=[pltpu.VMEM((8, 4, ROWS, w), BF16) for w in WIDTHS]
        + [pltpu.VMEM((8, 4, ROWS, CH), BF16)]
        + [pltpu.VMEM((ROWS, w), BF16) for w in WIDTHS]
        + [
            pltpu.VMEM((TOK, D), BF16),
            pltpu.VMEM((4, 8, TOK, COLS), BF16),
            pltpu.VMEM((4, TOK, D), BF16),
            pltpu.VMEM((4, TOK, CH), BF16),
            pltpu.VMEM((2, TOK, CH), BF16),
            pltpu.VMEM((4, TOK, HID), BF16),
            pltpu.VMEM((4 * TOK, 3 * CH), F32),
            pltpu.VMEM((2, NCOL, TOK, COLS), BF16),
            pltpu.VMEM((2, NCOL, TOK, COLS), BF16),
            pltpu.VMEM((NCOL, TOK, COLS), BF16),
            pltpu.VMEM((NCOL, TOK, COLS), BF16),
            pltpu.VMEM((NCOL, TOK, COLS), F32),
            pltpu.VMEM((2, 2, TOK, COLS), F32),
            dma((8,)),
            dma((3, 2)),
            dma((3, 2, 20)),
            dma((3, 2)),
            dma((3, 2)),
            dma,
            dma((3,)),
            dma((7,)),
            dma((3,)),
            dma((3, 3)),
            dma((4, 2)),
            dma((4, 2)),
            dma((2,)),
            dma((2,)),
            dma((2, 2)),
            dma((2, 2, 24)),
            dma,
            dma((24,)),
            dma((3,)),
        ],
        compiler_params=pltpu.CompilerParams(
            collective_id=0, has_side_effects=True, vmem_limit_bytes=67_043_328
        ),
    )(
        tokens, outer_weight, inner_weight, value_weight, mix_out.T, up_weight, down_weight.T,
        conv_taps, norm_first.reshape(1, D), norm_second.reshape(1, D),
    )


def solution(mesh):
    finer = Mesh(
        mesh.devices.reshape(mesh.shape["rep"], 2, 4, 4, mesh.shape["tp"]),
        ("rep", "fs_0", "fs_1", "fs_2", "tp"),
    )
    placed = (
        P(REP_FS_TP, None),
        P(FS, "tp"),
        P(FS, "tp"),
        P(FS, "tp"),
        P(None, "tp"),
        P("tp", FS),
        P(),
        P(FS, "tp"),
        P("tp", FS),
        P(),
    )
    return jax.shard_map(
        local, mesh=finer, in_specs=placed, out_specs=P(REP_FS_TP, None), check_vma=False
    )
```

time: 128 us -> 113 us (0.88)
  Pallas kernels: 125 us -> 110 us
    pallas_call x1, Pallas kernels: 125 us -> 110 us  [local(): pl.pallas_call(kernel, name='mixer_ffn', out_shape=jax.ShapeDtypeStruct((...]
where the time goes in v4:
time: 113 us
  Pallas kernels  110 us (97%)
  local copies, waits for them, and re-layouts  2.73 us (2%)
    pallas_call x1, Pallas kernels, local(): pl.pallas_call(kernel, name='mixer_ffn', out_shape=jax.ShapeDtypeStruct((...  110 us
    unnamed x1, local copies, waits for them, and re-layouts  2.73 us

profile of v4, /device:TPU:0, one launch (start us, length us, event | category | flops | bytes accessed | tf_op | source)
XLA Modules:
  0.0 113.0 jit_solution(8558628986135878374)
XLA Ops:
  0.0 110.2 %mixer_ffn.1 = bf16[384,2048]{1,0:T(8,128)(2,1)} custom-call(bf16[384,2048]{1,0:T(8,128)(2,1)} %tok.1, f32[64,768]{1,0:T(8,128)} %wo_in.1, f32[64,768]{1,0:T(8,128)} %wi_in.1, f32[64,768]{1,0:T(8,128)} %wv_in.1, f32[64,768]{1,0:T(8,128)} %bitcast.5, f32[64,2048]{1,0:T(8,128)} %wu_in.1, f32[64,2048]{1,0:T(8,128)} %bitcast.4, f32[3,768]{1,0:T(4,128)} %taps.1, ...), custom_call_target="tpu_custom_call" | custom-call | tf_op jit(solution)/shard_map/mixer_ffn/pallas_call | solution.py:530
  110.2 2.7 %copy.12 = bf16[384,2048]{1,0:T(8,128)(2,1)} copy(bf16[384,2048]{1,0:T(8,128)(2,1)} %mixer_ffn.1) | data formatting | bytes 3145728

commit v5 on v4

--- a/solution.py
+++ b/solution.py
@@ -68,13 +68,16 @@
             source = (wo_in, wi_in, wv_in, wm_in)[which]
         else:
             source = (wu_in, wd_in)[which // 2 - 2].at[:, pl.ds(which % 2 * HID, HID)]
-        return pltpu.make_async_copy(source, stage(which, 2 * CH if which < 4 else HID), s_in.at[which])
+        return pltpu.make_async_copy(source, stage(which, 2 * CH if which < 4 else HID), s_in.at[max(which // 2 - 1, 0)])
+
+    def loaded(t):
+        part = pd.at[(pl.ds(0, 4 * ROWS), pl.ds(0, 2 * CH))] if t == MIXER else pd.at[pl.ds(2 * ROWS, 2 * ROWS), pl.ds(0, HID)]
+        pltpu.make_async_copy(part, part, s_in.at[t]).wait()
 
     def cast(t):
         keep, give = weights[t].at[own_row[0], own_row[1]], given[t]
         if t == MIXER:
-            for which in range(4):
-                load(which).wait()
+            loaded(t)
             pieces = [(i, c0, at + i * width, width) for width, c0, at in ((256, 0, 0), (128, 256, 768)) for i in range(3)]
             for i, c0, at, width in pieces + [(3, 0, 3 * CH, CH)]:
                 kept = pl.ds(pl.multiple_of(zl * CH + c0, 128), width)
@@ -83,8 +86,7 @@
                 give[:, at:at + width] = pd[i * ROWS:(i + 1) * ROWS, passed].astype(BF16)
         else:
             first = 2 + 2 * t
-            load(first).wait()
-            load(first + 1).wait()
+            loaded(t)
             keep[...] = stage(first + zl, HID)[...].astype(BF16)
             give[...] = stage(first + 1 - zl, HID)[...].astype(BF16)
 
@@ -101,27 +103,28 @@
         along_y = color if leg == 1 else 1 - color
         return device(z, (my_y + step * along_y) % 4, (my_x + step * (1 - along_y)) % 4, core)
 
-    def wcopy(t, color, slot, row, start, rows, target):
+    def wcopy(t, color, slot, row, start, rows, target, sent=0):
         part = weights[t].at[row[0], row[1], pl.ds(start, rows)]
-        return remote(part, part, sw_send.at[t, int(slot == 0)], sw_recv.at[t, color, slot], target)
-
-    def arrive(t, color, slot, row, start, rows):
-        wcopy(t, color, slot, row, start, rows, x_plus).wait_recv()
+        return remote(part, part, sw_send.at[t, sent], sw_recv.at[t, color, slot], target)
+
+    def arrive(t, color, slot, blocks):
+        part = weights[t].at[0, pl.ds(0, blocks)]
+        remote(part, part, sw_send.at[t, 0], sw_recv.at[t, color, slot], x_plus).wait_recv()
 
     def first_leg(t, color):
         row = block(color, 0, 0)
-        wcopy(t, color, 0, row, 0, ROWS, ring(color, 1, 1)).start()
-        wcopy(t, color, 1, row, 0, ROWS, ring(color, 1, 3)).start()
+        wcopy(t, color, 0, row, 0, ROWS, ring(color, 1, 1), 1).start()
+        wcopy(t, color, 0, row, 0, ROWS, ring(color, 1, 3)).start()
 
     def second_leg(t, color, k):
         row = block(color, k, 0)
-        wcopy(t, color, 4 + 4 * k, row, 0, ROWS, ring(color, 2, 1)).start()
-        wcopy(t, color, 5 + 4 * k, row, 0, ROWS, ring(color, 2, 3)).start()
+        wcopy(t, color, 2 + k, row, 0, ROWS, ring(color, 2, 1)).start()
+        wcopy(t, color, 2 + k, row, 0, ROWS, ring(color, 2, 3)).start()
 
     def zcopy(t, half, row, target):
         return remote(
             given[t].at[pl.ds(half * HALF, HALF)], weights[t].at[row[0], row[1], pl.ds(half * HALF, HALF)],
-            sz_send.at[t, half], sz_recv.at[t, half], target,
+            sz_send.at[t], sz_recv.at[t], target,
         )
 
     def start_z(t):
@@ -129,36 +132,25 @@
         zcopy(t, 1, own_row, below).start()
 
     def z_arrived(t):
-        zcopy(t, 0, other_row, above).wait_recv()
-        zcopy(t, 1, other_row, below).wait_recv()
+        part = weights[t].at[other_row[0], other_row[1]]
+        remote(part, part, sz_send.at[t], sz_recv.at[t], above).wait_recv()
 
     def g1(t, color):
-        row = block(color, 1, 0)
-        arrive(t, color, 0, row, 0, ROWS)
-        wcopy(t, color, 2, row, 0, HALF, ring(color, 1, 1)).start()
-        row = block(color, 2, 0)
-        arrive(t, color, 1, row, 0, ROWS)
-        wcopy(t, color, 3, row, HALF, HALF, ring(color, 1, 3)).start()
+        arrive(t, color, 0, 2)
+        wcopy(t, color, 1, block(color, 1, 0), 0, HALF, ring(color, 1, 1)).start()
+        wcopy(t, color, 1, block(color, 2, 0), HALF, HALF, ring(color, 1, 3)).start()
 
     def g2(t, color):
-        row = block(color, 3, 0)
-        arrive(t, color, 2, row, 0, HALF)
-        arrive(t, color, 3, row, HALF, HALF)
+        arrive(t, color, 1, 1)
 
     def g3(t, color, k):
-        row = block(color, k, 1)
-        arrive(t, color, 4 + 4 * k, row, 0, ROWS)
-        wcopy(t, color, 6 + 4 * k, row, 0, HALF, ring(color, 2, 1)).start()
-        row = block(color, k, 2)
-        arrive(t, color, 5 + 4 * k, row, 0, ROWS)
-        wcopy(t, color, 7 + 4 * k, row, HALF, HALF, ring(color, 2, 3)).start()
+        arrive(t, color, 2 + k, 2)
+        wcopy(t, color, 6, block(color, k, 1), 0, HALF, ring(color, 2, 1)).start()
+        wcopy(t, color, 6, block(color, k, 2), HALF, HALF, ring(color, 2, 3)).start()
 
     def g4(t):
-        for k in range(4):
-            for color in (mine, theirs):
-                row = block(color, k, 3)
-                arrive(t, color, 6 + 4 * k, row, 0, HALF)
-                arrive(t, color, 7 + 4 * k, row, HALF, HALF)
+        for color in (mine, theirs):
+            arrive(t, color, 6, 4)
 
     def chunk(color, k):
         return ((my_y, my_x)[color] + SHIFT[k]) % 4
@@ -169,50 +161,53 @@
     def mix_swap(k, color):
         source = chunk_rows(wp, color, chunk(color, k)).at[:, :, pl.ds(3 * CH, CH)]
         return remote(
-            source, chunk_rows(wm2, color, chunk(color, k)), sq_send.at[k, color], sq_recv.at[k, color], (above, below)[color]
+            source, chunk_rows(wm2, color, chunk(color, k)), sq_send, sq_recv, (above, below)[color]
         )
 
     def seq(s):
         return pl.ds(s * SEQ, SEQ)
 
     def tok_z(s):
-        return remote(x.at[0, :, seq(s)], x.at[2, :, seq(s)], sx_send.at[0], sx_recv.at[1 + s], helper)
+        return remote(x.at[0, :, seq(s)], x.at[2, :, seq(s)], sx_send, sx_recv.at[1 + s], helper)
 
     def tok_sibling():
-        return remote(x.at[0], x.at[1], sx_send.at[1], sx_recv.at[0], sibling)
+        return remote(x.at[0], x.at[1], sx_send, sx_recv.at[0], sibling)
 
     def tok_relay(s):
-        return remote(x.at[2, :, seq(s)], x.at[3, :, seq(s)], sx_send.at[2], sx_recv.at[4 + s], sibling)
+        return remote(x.at[2, :, seq(s)], x.at[3, :, seq(s)], sx_send, sx_recv.at[4], sibling)
 
     def first_copy(kind, s):
         source, target, to = ((0, 1, sibling), (0, 2, helper), (2, 3, sibling))[kind]
-        return remote(f.at[source, seq(s)], f.at[target, seq(s)], sf_send.at[kind], sf_recv.at[kind, s], to)
+        return remote(f.at[source, seq(s)], f.at[target, seq(s)], sf_send, sf_recv.at[(0, 1 + s, 4 + s)[kind]], to)
 
     def mixed_copy(i):
-        return remote(mixed.at[2 + i], mixed2.at[i], sm_send.at[i], sm_recv.at[i], (helped, helper)[i])
+        return remote(mixed.at[2 + i], mixed2.at[i], sm_send, sm_recv, (helped, helper)[i])
 
     def mix_copy(s):
         rows = (0, slice(None), seq(s))
-        return remote(d_send.at[rows], d_recv.at[rows], sd_send.at[0, 0], sd_recv.at[0, 0, s], sibling)
+        return remote(d_send.at[rows], d_recv.at[rows], sd_send.at[0], sd_recv.at[s], sibling)
 
     def piece(k, color, s):
-        j = color * 4 + chunk(color, k)
-        return j, pl.ds(0, TOK) if s is None else seq(s), (k * 2 + color) * NSEQ + (s or 0)
+        return color * 4 + chunk(color, k), pl.ds(0, TOK) if s is None else seq(s)
 
     def part_copy(slot, k, color, s=None):
-        j, rows, at = piece(k, color, s)
-        return remote(d_send.at[slot, j, rows], d_recv.at[slot, j, rows], sd_send.at[1, slot], sd_recv.at[1, slot, at], sibling)
+        j, rows = piece(k, color, s)
+        at = 3 if slot == 0 else 4 + 3 * k + s if k < 2 else 8 + k
+        return remote(d_send.at[slot, j, rows], d_recv.at[slot, j, rows], sd_send.at[1], sd_recv.at[at], sibling)
 
     def sum_copy(k, color, s=None):
-        j, rows, at = piece(k, color, s)
-        return remote(z_send.at[j, rows], z_recv.at[j, rows], sr_send, sr_recv.at[at], helped)
+        j, rows = piece(k, color, s)
+        return remote(z_send.at[j, rows], z_recv.at[j, rows], sr_send, sr_recv.at[0 if k < 3 else 1 + s], helped)
+
+    def came(ref, sem):
+        remote(ref, ref, sr_send, sem, x_plus).wait_recv()
 
     def relay_tokens(s):
         tok_z(s).wait_recv()
         tok_relay(s).start()
 
     def all_sent(ref, sem):
-        remote(ref, ref, sem, sw_recv.at[0, 0, 0], x_plus).wait_send()
+        remote(ref, ref, sem, sr_recv.at[0], x_plus).wait_send()
 
     row_id = lax.broadcasted_iota(jnp.int32, (SEQ, 1), 0)
 
@@ -289,11 +284,11 @@
             part_copy(p, k, color, s).start()
 
     def ffn_send(k, s=None):
+        if k < 3:
+            rows = pl.ds(0, TOK) if s is None else seq(s)
+            came(d_recv.at[1, pl.ds(0, 2), rows], sd_recv.at[4 + 3 * k + s if k < 2 else 8 + k])
         for color in (0, 1):
-            if k < 3:
-                part_copy(1, k, color, s).wait_recv()
-        for color in (0, 1):
-            j, rows, _ = piece(k, color, s)
+            j, rows = piece(k, color, s)
             z_send[j, rows, :] = (held[k % 2, color, rows, :] + d_recv[1, j, rows, :].astype(F32)).astype(BF16)
         for color in (0, 1):
             sum_copy(k, color, s).start()
@@ -388,8 +383,7 @@
     each(g3, MIXER, 1)
     relay_tokens(2)
     each(g3, MIXER, 2)
-    for s in range(NSEQ):
-        tok_relay(s).wait_recv()
+    came(x.at[3], sx_recv.at[4])
     project(1, 0)
     each(g3, MIXER, 3)
     z_arrived(UP)
@@ -421,13 +415,8 @@
     project(0, 3)
     convolve(1)
     convolve(0)
-    each(g1, DOWN)
-    each(g3, UP, 1)
-    for k in range(4):
-        for color in (0, 1):
-            mix_swap(k, color).wait_recv()
-    mixed_copy(1).wait_recv()
-    mixed_copy(0).wait_recv()
+    came(wm2, sq_recv)
+    came(mixed2, sm_recv)
 
     def mixing(rows):
         return jnp.concatenate([acc[j, rows, :] + d_recv[0, j, rows, :].astype(F32) for j in range(NCOL)], axis=1)
@@ -439,88 +428,91 @@
         first_copy(0, s).start()
 
     mix_sums(0)
-    each(g3, UP, 2)
+    each(g3, UP, 1)
     mix_sums(1)
     make_first(0)
+    each(g1, DOWN)
     mix_sums(2)
+    each(g3, UP, 2)
+    make_first(1)
+    second_leg(DOWN, mine, 0)
+    second_leg(DOWN, theirs, 0)
+    make_first(2)
     each(g3, UP, 3)
-    for k in (0, 1, 2):
+    for k in (1, 2):
         each(second_leg, DOWN, k)
-    make_first(1)
-    make_first(2)
     each(g2, DOWN)
     each(second_leg, DOWN, 3)
+    came(f.at[1], sf_recv.at[0])
     g4(UP)
     expand(0)
     each(g3, DOWN, 0)
-    for s in range(NSEQ):
-        first_copy(0, s).wait_recv()
+    all_sent(d_send.at[0], sd_send.at[0])
+    first_copy(1, 0).wait_recv()
+    first_copy(2, 0).start()
+    expand(2, 0)
+    first_copy(2, 0).wait_recv()
+    expand(3, 0)
+    ffn_sums(1, 0, 0)
     expand(1)
-    all_sent(d_send.at[0], sd_send.at[0, 0])
-    for s in range(NSEQ):
-        first_copy(1, s).wait_recv()
-        first_copy(2, s).start()
-        expand(2, s)
-        if s > 0:
-            ffn_send(0, s - 1)
-        first_copy(2, s).wait_recv()
-        expand(3, s)
-        ffn_sums(1, 0, s)
-        each(g3, DOWN, s + 1)
-    ffn_sums(1, 1)
+    ffn_send(0, 0)
+    each(g3, DOWN, 1)
+    first_copy(1, 1).wait_recv()
+    first_copy(2, 1).start()
+    expand(2, 1)
+    each(g3, DOWN, 2)
+    first_copy(2, 1).wait_recv()
+    expand(3, 1)
+    ffn_sums(1, 0, 1)
+    each(g3, DOWN, 3)
+    ffn_sums(1, 1, 0)
+    ffn_send(0, 1)
+    ffn_sums(1, 1, 1)
+    ffn_send(1, 0)
+    first_copy(1, 2).wait_recv()
+    first_copy(2, 2).start()
+    expand(2, 2)
+    ffn_send(1, 1)
+    first_copy(2, 2).wait_recv()
+    expand(3, 2)
+    ffn_sums(1, 0, 2)
+    ffn_sums(1, 1, 2)
     ffn_send(0, 2)
     ffn_sums(1, 2)
-    ffn_send(1)
-    ffn_sums(0, 0)
-    ffn_send(2)
+    ffn_send(1, 2)
     g4(DOWN)
     ffn_sums(1, 3)
-    ffn_sums(0, 1)
-    for color in (0, 1):
-        part_copy(1, 3, color).wait_recv()
+    ffn_send(2)
+    ffn_sums(0, 0)
+    came(d_recv.at[1, pl.ds(0, 2)], sd_recv.at[11])
     for s in range(NSEQ):
         ffn_send(3, s)
-    ffn_sums(0, 2)
-    ffn_sums(0, 3)
-    for k in range(4):
-        for color in (0, 1):
-            part_copy(0, k, color).wait_recv()
-            if k == 0:
-                for s in range(NSEQ):
-                    sum_copy(k, color, s).wait_recv()
-            elif k < 3:
-                sum_copy(k, color).wait_recv()
+    for k in (1, 2, 3):
+        ffn_sums(0, k)
+    came(d_recv.at[0], sd_recv.at[3])
+    came(z_recv.at[pl.ds(0, 6)], sr_recv.at[0])
 
     def lowered(rows):
         return natural([
             acc[j, rows, :] + d_recv[0, j, rows, :].astype(F32) + z_recv[j, rows, :].astype(F32) for j in range(NCOL)
         ])
 
-    results = []
     for s in range(NSEQ):
-        for color in (0, 1):
-            sum_copy(3, color, s).wait_recv()
+        came(z_recv.at[pl.ds(0, 2), seq(s)], sr_recv.at[1 + s])
         normed(f.at[0], lowered, gain2, s, own)
-        results.append(pltpu.make_async_copy(own.at[seq(s)], out.at[seq(s)], s_out.at[s]))
-        results[-1].start()
+        pltpu.make_async_copy(own.at[seq(s)], out.at[seq(s)], s_out).start()
 
     for t in range(3):
         all_sent(weights[t].at[pl.ds(0, 7)], sw_send.at[t, 0])
         all_sent(weights[t].at[0, pl.ds(0, 2)], sw_send.at[t, 1])
-        zcopy(t, 0, own_row, above).wait_send()
-        zcopy(t, 1, own_row, below).wait_send()
-    for kind in range(3):
-        all_sent(x.at[0], sx_send.at[kind])
-        all_sent(f.at[0], sf_send.at[kind])
-    for k in range(4):
-        for color in (0, 1):
-            mix_swap(k, color).wait_send()
-    for i in (0, 1):
-        mixed_copy(i).wait_send()
-        all_sent(d_send.at[i], sd_send.at[1, i])
+        all_sent(given[t], sz_send.at[t])
+    all_sent(x.at[pl.ds(0, 3)], sx_send)
+    all_sent(f.at[pl.ds(0, 3)], sf_send)
+    all_sent(wm2, sq_send)
+    all_sent(mixed2, sm_send)
+    all_sent(d_send, sd_send.at[1])
     all_sent(z_send, sr_send)
-    for result in results:
-        result.wait()
+    pltpu.make_async_copy(own, out, s_out).wait()
 
 
 def local(tokens, outer_weight, inner_weight, value_weight, conv_taps, mix_out, norm_first, up_weight, down_weight, norm_second):
@@ -550,25 +542,25 @@
             pltpu.VMEM((NCOL, TOK, COLS), BF16),
             pltpu.VMEM((NCOL, TOK, COLS), F32),
             pltpu.VMEM((2, 2, TOK, COLS), F32),
-            dma((8,)),
+            dma((3,)),
             dma((3, 2)),
-            dma((3, 2, 20)),
-            dma((3, 2)),
-            dma((3, 2)),
-            dma,
+            dma((3, 2, 7)),
             dma((3,)),
+            dma((3,)),
+            dma,
+            dma,
+            dma((5,)),
+            dma,
             dma((7,)),
-            dma((3,)),
-            dma((3, 3)),
-            dma((4, 2)),
-            dma((4, 2)),
+            dma,
+            dma,
+            dma,
+            dma,
             dma((2,)),
-            dma((2,)),
-            dma((2, 2)),
-            dma((2, 2, 24)),
-            dma,
-            dma((24,)),
-            dma((3,)),
+            dma((12,)),
+            dma,
+            dma((4,)),
+            dma,
         ],
         compiler_params=pltpu.CompilerParams(
             collective_id=0, has_side_effects=True, vmem_limit_bytes=67_043_328

time: 113 us -> 106 us (0.938)
  Pallas kernels: 110 us -> 103 us
    pallas_call x1, Pallas kernels: 110 us -> 103 us  [local(): pl.pallas_call(kernel, name='mixer_ffn', out_shape=jax.ShapeDtypeStruct((...]
where the time goes in v5:
time: 106 us
  Pallas kernels  103 us (97%)
  local copies, waits for them, and re-layouts  2.73 us (3%)
    pallas_call x1, Pallas kernels, local(): pl.pallas_call(kernel, name='mixer_ffn', out_shape=jax.ShapeDtypeStruct((...  103 us
    unnamed x1, local copies, waits for them, and re-layouts  2.73 us

profile of v5, /device:TPU:0, one launch (start us, length us, event | category | flops | bytes accessed | tf_op | source)
XLA Modules:
  0.0 105.9 jit_solution(3632889470043201603)
XLA Ops:
  0.0 103.2 %mixer_ffn.1 = bf16[384,2048]{1,0:T(8,128)(2,1)} custom-call(bf16[384,2048]{1,0:T(8,128)(2,1)} %tok.1, f32[64,768]{1,0:T(8,128)} %wo_in.1, f32[64,768]{1,0:T(8,128)} %wi_in.1, f32[64,768]{1,0:T(8,128)} %wv_in.1, f32[64,768]{1,0:T(8,128)} %bitcast.5, f32[64,2048]{1,0:T(8,128)} %wu_in.1, f32[64,2048]{1,0:T(8,128)} %bitcast.4, f32[3,768]{1,0:T(4,128)} %taps.1, ...), custom_call_target="tpu_custom_call" | custom-call | tf_op jit(solution)/shard_map/mixer_ffn/pallas_call | solution.py:522
  103.2 2.7 %copy.12 = bf16[384,2048]{1,0:T(8,128)(2,1)} copy(bf16[384,2048]{1,0:T(8,128)(2,1)} %mixer_ffn.1) | data formatting | bytes 3145728

commit v6 on v5

--- a/solution.py
+++ b/solution.py
@@ -28,11 +28,11 @@
 
 
 def kernel(
-    tok, wo_in, wi_in, wv_in, wm_in, wu_in, wd_in, taps, gain1, gain2, out,
+    tok, wo_in, wi_in, wv_in, wm_in, wu_in, wd_in, taps_in, gain1_in, gain2_in, own,
     wp, wu, wd, wm2, gp, gu, gd,
-    own, x, f, mixed, mixed2, hid, pd, d_send, d_recv, z_send, z_recv, acc, held,
-    s_in, sw_send, sw_recv, sz_send, sz_recv, sx_own, sx_send, sx_recv, sf_send, sf_recv,
-    sq_send, sq_recv, sm_send, sm_recv, sd_send, sd_recv, sr_send, sr_recv, s_out,
+    x, f, mixed, mixed2, hid, pd, d_send, d_recv, z_send, z_recv, acc, held, taps, gain1, gain2,
+    s_small, s_in, sw_send, sw_recv, sz_send, sz_recv, sx_own, sx_send, sx_recv, sf_send, sf_recv,
+    sq_send, sq_recv, sm_send, sm_recv, sd_send, sd_recv, sr_send, sr_recv,
 ):
     rep, zl = lax.axis_index("rep"), lax.axis_index("fs_0")
     my_y, my_x, core = lax.axis_index("fs_1"), lax.axis_index("fs_2"), lax.axis_index("tp")
@@ -338,11 +338,14 @@
     own_tokens.start()
     for which in range(4, 8):
         load(which).start()
+
+    def small_loads(wait):
+        for i, (source, target) in enumerate(((taps_in, taps), (gain1_in, gain1), (gain2_in, gain2))):
+            copy = pltpu.make_async_copy(source, target, s_small.at[i])
+            copy.wait() if wait else copy.start()
+
+    small_loads(False)
     cast(MIXER)
-    own_tokens.wait()
-    spread_tokens()
-    cast(UP)
-    cast(DOWN)
     pl.semaphore_wait(barrier, 7)
 
     both = (mine, theirs)
@@ -354,12 +357,17 @@
     start_z(MIXER)
     first_leg(MIXER, mine)
     second_leg(MIXER, mine, 0)
+    own_tokens.wait()
+    spread_tokens()
     tok_z(0).start()
     tok_sibling().start()
+    cast(UP)
     start_z(UP)
     tok_z(1).start()
     tok_z(2).start()
+    cast(DOWN)
     start_z(DOWN)
+    small_loads(True)
     z_arrived(MIXER)
     first_leg(MIXER, theirs)
     second_leg(MIXER, theirs, 0)
@@ -500,7 +508,6 @@
     for s in range(NSEQ):
         came(z_recv.at[pl.ds(0, 2), seq(s)], sr_recv.at[1 + s])
         normed(f.at[0], lowered, gain2, s, own)
-        pltpu.make_async_copy(own.at[seq(s)], out.at[seq(s)], s_out).start()
 
     for t in range(3):
         all_sent(weights[t].at[pl.ds(0, 7)], sw_send.at[t, 0])
@@ -512,7 +519,6 @@
     all_sent(mixed2, sm_send)
     all_sent(d_send, sd_send.at[1])
     all_sent(z_send, sr_send)
-    pltpu.make_async_copy(own, out, s_out).wait()
 
 
 def local(tokens, outer_weight, inner_weight, value_weight, conv_taps, mix_out, norm_first, up_weight, down_weight, norm_second):
@@ -522,14 +528,13 @@
     return pl.pallas_call(
         kernel,
         name="mixer_ffn",
-        out_shape=jax.ShapeDtypeStruct((TOK, D), BF16),
-        in_specs=[hbm] * 7 + [vmem] * 3,
-        out_specs=hbm,
+        out_shape=pltpu.VMEM((TOK, D), BF16),
+        in_specs=[hbm] * 10,
+        out_specs=vmem,
         scratch_shapes=[pltpu.VMEM((8, 4, ROWS, w), BF16) for w in WIDTHS]
         + [pltpu.VMEM((8, 4, ROWS, CH), BF16)]
         + [pltpu.VMEM((ROWS, w), BF16) for w in WIDTHS]
         + [
-            pltpu.VMEM((TOK, D), BF16),
             pltpu.VMEM((4, 8, TOK, COLS), BF16),
             pltpu.VMEM((4, TOK, D), BF16),
             pltpu.VMEM((4, TOK, CH), BF16),
@@ -542,6 +547,10 @@
             pltpu.VMEM((NCOL, TOK, COLS), BF16),
             pltpu.VMEM((NCOL, TOK, COLS), F32),
             pltpu.VMEM((2, 2, TOK, COLS), F32),
+            pltpu.VMEM((3, 2 * CH), F32),
+            pltpu.VMEM((1, D), F32),
+            pltpu.VMEM((1, D), F32),
+            dma((3,)),
             dma((3,)),
             dma((3, 2)),
             dma((3, 2, 7)),
@@ -560,10 +569,9 @@
             dma((12,)),
             dma,
             dma((4,)),
-            dma,
         ],
         compiler_params=pltpu.CompilerParams(
-            collective_id=0, has_side_effects=True, vmem_limit_bytes=67_043_328
+            collective_id=0, has_side_effects=True, vmem_limit_bytes=62 * 1024 * 1024
         ),
     )(
         tokens, outer_weight, inner_weight, value_weight, mix_out.T, up_weight, down_weight.T,

time: 106 us -> 103 us (0.972)
  local copies, waits for them, and re-layouts: 2.73 us -> 1.15 us
    unnamed x1, local copies, waits for them, and re-layouts: 2.73 us -> 1.15 us
    pallas_call x1, Pallas kernels: 103 us -> 102 us  [local(): pl.pallas_call(kernel, name='mixer_ffn', out_shape=pltpu.VMEM((TOK, D), B...]
where the time goes in v6:
time: 103 us
  Pallas kernels  102 us (99%)
  local copies, waits for them, and re-layouts  1.15 us (1%)
    pallas_call x1, Pallas kernels, local(): pl.pallas_call(kernel, name='mixer_ffn', out_shape=pltpu.VMEM((TOK, D), B...  102 us

profile of v6, /device:TPU:0, one launch (start us, length us, event | category | flops | bytes accessed | tf_op | source)
XLA Modules:
  0.0 102.9 jit_solution(18017607655446852362)
XLA Ops:
  0.0 101.7 %mixer_ffn.1 = bf16[384,2048]{1,0:T(8,128)(2,1)S(1)} custom-call(bf16[384,2048]{1,0:T(8,128)(2,1)} %tok.1, f32[64,768]{1,0:T(8,128)} %wo_in.1, f32[64,768]{1,0:T(8,128)} %wi_in.1, f32[64,768]{1,0:T(8,128)} %wv_in.1, f32[64,768]{1,0:T(8,128)} %bitcast.5, f32[64,2048]{1,0:T(8,128)} %wu_in.1, f32[64,2048]{1,0:T(8,128)} %bitcast.4, f32[3,768]{1,0:T(4,128)} %taps_in.1, ...), custom_call_target="tpu_custom_call" | custom-call | tf_op jit(solution)/shard_map/mixer_ffn/pallas_call | solution.py:528
  101.7 1.1 %copy.12 = bf16[384,2048]{1,0:T(8,128)(2,1)} copy(bf16[384,2048]{1,0:T(8,128)(2,1)S(1)} %mixer_ffn.1) | data formatting | bytes 3145728

commit v7 on v6

--- a/solution.py
+++ b/solution.py
@@ -316,7 +316,7 @@
             target[rows, :] = (center * lax.rsqrt(spread + EPS) * gain[...]).astype(BF16)
             return 0
 
-        lax.fori_loop(0, SEQ // step_rows, step, 0)
+        lax.fori_loop(0, SEQ // step_rows, step, 0, unroll=2)
 
     def expand(g, s=None):
         rows = pl.ds(0, TOK) if s is None else seq(s)
@@ -452,33 +452,31 @@
     each(g2, DOWN)
     each(second_leg, DOWN, 3)
     came(f.at[1], sf_recv.at[0])
-    g4(UP)
-    expand(0)
-    each(g3, DOWN, 0)
-    all_sent(d_send.at[0], sd_send.at[0])
     first_copy(1, 0).wait_recv()
     first_copy(2, 0).start()
+    g4(UP)
     expand(2, 0)
     first_copy(2, 0).wait_recv()
     expand(3, 0)
     ffn_sums(1, 0, 0)
-    expand(1)
-    ffn_send(0, 0)
-    each(g3, DOWN, 1)
+    each(g3, DOWN, 0)
     first_copy(1, 1).wait_recv()
     first_copy(2, 1).start()
     expand(2, 1)
+    ffn_send(0, 0)
+    each(g3, DOWN, 1)
+    expand(0)
     each(g3, DOWN, 2)
     first_copy(2, 1).wait_recv()
     expand(3, 1)
     ffn_sums(1, 0, 1)
     each(g3, DOWN, 3)
+    first_copy(1, 2).wait_recv()
+    first_copy(2, 2).start()
     ffn_sums(1, 1, 0)
     ffn_send(0, 1)
     ffn_sums(1, 1, 1)
     ffn_send(1, 0)
-    first_copy(1, 2).wait_recv()
-    first_copy(2, 2).start()
     expand(2, 2)
     ffn_send(1, 1)
     first_copy(2, 2).wait_recv()
@@ -488,9 +486,11 @@
     ffn_send(0, 2)
     ffn_sums(1, 2)
     ffn_send(1, 2)
+    expand(1)
+    ffn_send(2)
     g4(DOWN)
     ffn_sums(1, 3)
-    ffn_send(2)
+    all_sent(d_send.at[0], sd_send.at[0])
     ffn_sums(0, 0)
     came(d_recv.at[1, pl.ds(0, 2)], sd_recv.at[11])
     for s in range(NSEQ):

time: 103 us -> 102 us (level)
  Pallas kernels: 102 us -> 99.9 us
    pallas_call x1, Pallas kernels: 102 us -> 99.9 us  [local(): pl.pallas_call(kernel, name='mixer_ffn', out_shape=pltpu.VMEM((TOK, D), B...]
where the time goes in v7:
time: 102 us; the launch traced here: 101 us
  Pallas kernels  99.9 us (98%)
  local copies, waits for them, and re-layouts  1.15 us (1%)
    pallas_call x1, Pallas kernels, local(): pl.pallas_call(kernel, name='mixer_ffn', out_shape=pltpu.VMEM((TOK, D), B...  99.9 us

profile of v7, /device:TPU:0, one launch (start us, length us, event | category | flops | bytes accessed | tf_op | source)
XLA Modules:
  0.0 101.0 jit_solution(16076435894955418333)
XLA Ops:
  0.0 99.9 %mixer_ffn.1 = bf16[384,2048]{1,0:T(8,128)(2,1)S(1)} custom-call(bf16[384,2048]{1,0:T(8,128)(2,1)} %tok.1, f32[64,768]{1,0:T(8,128)} %wo_in.1, f32[64,768]{1,0:T(8,128)} %wi_in.1, f32[64,768]{1,0:T(8,128)} %wv_in.1, f32[64,768]{1,0:T(8,128)} %bitcast.5, f32[64,2048]{1,0:T(8,128)} %wu_in.1, f32[64,2048]{1,0:T(8,128)} %bitcast.4, f32[3,768]{1,0:T(4,128)} %taps_in.1, ...), custom_call_target="tpu_custom_call" | custom-call | tf_op jit(solution)/shard_map/mixer_ffn/pallas_call | solution.py:528
  99.9 1.1 %copy.12 = bf16[384,2048]{1,0:T(8,128)(2,1)} copy(bf16[384,2048]{1,0:T(8,128)(2,1)S(1)} %mixer_ffn.1) | data formatting | bytes 3145728
